TPU v7x, 256 devices: a whole 4x4x8 slice. The times are simulated.
256 devices in a mesh: ep: 32 (over z, x), tp: 8 (over y, core).
Axes of the slice: x: 4, y: 4, z: 8, core: 2. Of those that a mesh axis runs over, the one named last changes fastest.
Arguments:
- mixer_input: bfloat16 [4096, 2048], P('ep'), may hold values from -6 to 6
- mixer_gain: bfloat16 [2048], replicated, may hold values from 0.099609375 to 1.8984375
- query_matrix: bfloat16 [2048, 2048], P(None, 'tp'), may hold values from -0.125 to 0.125
- key_matrix: bfloat16 [2048, 2048], P(None, 'tp'), may hold values from -0.125 to 0.125
- value_matrix: bfloat16 [2048, 2048], P(None, 'tp'), may hold values from -0.125 to 0.125
- decay_down_factor: bfloat16 [2048, 64], replicated, may hold values from -0.125 to 0.125
- decay_up_factor: bfloat16 [64, 2048], P(None, 'tp'), may hold values from -1.1953125 to 1.1953125
- decay_bias_base: float32 [2048], P('tp'), may hold values from -16 to 0
- decay_shift: float32 [4096, 2048], P('ep', 'tp'), may hold values from -1.5 to 1.5
- decay_spike: float32 [4096, 2048], P('ep', 'tp'), may hold values from -1.4 to 0
- correction_rate_down: bfloat16 [2048, 64], replicated, may hold values from -0.125 to 0.125
- correction_rate_up: bfloat16 [64, 2048], P(None, 'tp'), may hold values from -1.1953125 to 1.1953125
- correction_rate_base: float32 [2048], P('tp'), may hold values from -8 to 1
- head_norm_gain: bfloat16 [2048], P('tp'), may hold values from 0.099609375 to 1.8984375
- output_weight: bfloat16 [2048, 2048], P('tp'), may hold values from -0.125 to 0.125
- feedforward_input: bfloat16 [8192, 2048], P(('ep', 'tp')), may hold values from -6 to 6
- feedforward_gain: bfloat16 [2048], replicated, may hold values from 0.099609375 to 1.8984375
- routed_expert_index: int32 [8192, 2], P('ep'), may hold values from 0 to 63, all different within a row; in each aligned block of 32 rows (0 to 31, 32 to 63, ...) at most 2 rows name the same one
- routed_expert_weight: float32 [8192, 2], P(('ep', 'tp')), may hold values from 0.3 to 2.5
- expert_gate_weight: bfloat16 [64, 2048, 1024], P('ep', None, 'tp'), may hold values from -0.125 to 0.125
- expert_up_weight: bfloat16 [64, 2048, 1024], P('ep', None, 'tp'), may hold values from -0.125 to 0.125
- expert_down_weight: bfloat16 [64, 1024, 2048], P('ep', 'tp'), may hold values from -0.1875 to 0.1875
- shared_gate_weight: bfloat16 [2048, 1024], P(None, 'tp'), may hold values from -0.125 to 0.125
- shared_up_weight: bfloat16 [2048, 1024], P(None, 'tp'), may hold values from -0.125 to 0.125
- shared_down_weight: bfloat16 [1024, 2048], P('tp'), may hold values from -0.1875 to 0.1875
Outputs:
- mixed_a: bfloat16 [4096, 2048], P(('ep', 'tp'))
- mixed_b: bfloat16 [8192, 2048], P(('ep', 'tp'))
Inputs may be any that keep to these rules, and one draw needn't show every extreme that they name: `routed_expert_index`: in each aligned block of 32 rows (the rows of one device) a row names 2 different experts and no expert is named more than 2 times; in every draw some block names some expert exactly 2 times.
All inputs are finite; a program needn't handle non-finite values.
Results may differ from a plain program's by a relative error of at most 0.017.
Values may be sent and summed in bfloat16 or wider, within the bound.
A program may use at most 128 MiB of HBM per device.

v0:
```python
import jax
import jax.numpy as jnp
from jax import lax
from jax.sharding import Mesh
from jax.sharding import PartitionSpec as P

HEAD = 64
TOP = 2
SPAN = 32
EP = ("ep_0", "ep_1")
EP_TP = ("ep_0", "ep_1", "tp")


norm_eps = 1e-06
group_eps = 0.00064
unit_eps = 1e-06


def filled_with(shard, identity):
    return jax.tree.map(
        lambda part, zero: jnp.zeros_like(part) + jnp.asarray(zero, part.dtype), shard, identity
    )


def prefix_by_axis(shard, axes, combine, identity):
    before = start = filled_with(shard, identity)
    total = shard
    for axis in reversed(axes):
        size, place = (lax.axis_size(axis), lax.axis_index(axis))
        pieces = jax.tree.map(
            lambda part, kind: lax.all_gather(part.astype(kind), axis),
            total,
            (jnp.bfloat16, jnp.bfloat16),
        )
        inside, total = (start, start)
        for k in range(size):
            passed = k < place
            total = combine(
                total, jax.tree.map(lambda part, own: part[k].astype(own.dtype), pieces, shard)
            )
            inside = jax.tree.map(lambda new, old: jnp.where(passed, new, old), total, inside)
        before = combine(inside, before)
    return before


def in_blocks(shard, dim, size):
    before, after = (shard.shape[:dim], shard.shape[dim + 1 :])
    return jnp.moveaxis(shard.reshape(*before, size, -1, *after), dim, 0)


def summed_on_arrival(shard, axis, dim):
    blocks = in_blocks(shard, dim, lax.axis_size(axis))
    arrived = lax.all_to_all(blocks, axis, split_axis=0, concat_axis=0, tiled=True)
    return arrived.astype(jnp.float32).sum(axis=0)


def sent_to_all(shard, axis):
    copies = jnp.broadcast_to(shard, (lax.axis_size(axis), *shard.shape))
    return lax.all_to_all(copies, axis, split_axis=0, concat_axis=0, tiled=True)


def laid_out(blocks, dim):
    dims = list(blocks.shape[1:])
    dims[dim] *= blocks.shape[0]
    return jnp.moveaxis(blocks, 0, dim).reshape(dims)


def gather_directly(shard, axis, dim):
    blocks = sent_to_all(shard, axis)
    return laid_out(blocks, dim)


def rms_rows(matrix, gain):
    values = matrix.astype(jnp.float32)
    scaled = values * lax.rsqrt(jnp.mean(values * values, axis=-1, keepdims=True) + norm_eps)
    return (scaled * gain.astype(jnp.float32)).astype(jnp.bfloat16)


def mixer_channel_rows(
    normed_rows,
    query_matrix,
    key_matrix,
    value_matrix,
    decay_down_factor,
    decay_up_factor,
    decay_bias_base,
    decay_shift,
    decay_spike,
    correction_rate_down,
    correction_rate_up,
    correction_rate_base,
):
    row_count = normed_rows.shape[0]
    head_count = query_matrix.shape[1] // HEAD

    def by_heads(matrix):
        return matrix.reshape(row_count, head_count, HEAD)

    query_matrix_rows = jnp.dot(normed_rows, query_matrix, preferred_element_type=jnp.float32)
    key_matrix_rows = jnp.dot(normed_rows, key_matrix, preferred_element_type=jnp.float32)
    value_matrix_rows = jnp.dot(normed_rows, value_matrix, preferred_element_type=jnp.float32)
    decay_low = jnp.tanh(
        jnp.dot(normed_rows, decay_down_factor, preferred_element_type=jnp.float32)
    ).astype(jnp.bfloat16)
    decay_logits = (
        decay_bias_base
        + jnp.dot(decay_low, decay_up_factor, preferred_element_type=jnp.float32)
        + decay_shift
    )
    logarithm_decay = decay_spike - jnp.exp(-jax.nn.softplus(-decay_logits) - 0.5)
    iclr_low = jnp.dot(
        normed_rows, correction_rate_down, preferred_element_type=jnp.float32
    ).astype(jnp.bfloat16)
    learning = jax.nn.sigmoid(
        correction_rate_base
        + jnp.dot(iclr_low, correction_rate_up, preferred_element_type=jnp.float32)
    )
    key_matrix_rows = by_heads(key_matrix_rows)
    unit_keys = key_matrix_rows * lax.rsqrt(
        jnp.sum(key_matrix_rows * key_matrix_rows, axis=-1, keepdims=True) + unit_eps
    )
    return (
        by_heads(query_matrix_rows),
        key_matrix_rows,
        by_heads(value_matrix_rows),
        -unit_keys,
        unit_keys * by_heads(learning),
        by_heads(logarithm_decay),
    )


def head_norm(outputs, gain):
    row_mean = jnp.mean(outputs, axis=-1, keepdims=True)
    centered = outputs - row_mean
    row_var = jnp.mean(centered * centered, axis=-1, keepdims=True)
    scaled = (centered * lax.rsqrt(row_var + group_eps)).reshape(outputs.shape[0], -1)
    return (scaled * gain.astype(jnp.float32)).astype(jnp.bfloat16)


def block_tables(query_matrix_rows, key_matrix_rows, erase_vector, write_vector, logarithm_decay):
    length = query_matrix_rows.shape[1]
    cumulative = jnp.cumsum(logarithm_decay, axis=1)
    before_decay = cumulative - logarithm_decay
    position = jnp.arange(length)
    strictly_below = (position[:, None] > position[None, :])[None, :, :, None]
    up_to = (position[:, None] >= position[None, :])[None, :, :, None]
    fade_before = jnp.exp(
        jnp.where(strictly_below, before_decay[:, :, None, :] - cumulative[:, None, :, :], -jnp.inf)
    )
    fade_upto = jnp.exp(
        jnp.where(up_to, cumulative[:, :, None, :] - cumulative[:, None, :, :], -jnp.inf)
    )
    erase_write = jnp.einsum("htc,htsc,hsc->hts", erase_vector, fade_before, write_vector)
    erase_key = jnp.einsum("htc,htsc,hsc->hts", erase_vector, fade_before, key_matrix_rows)
    query_write = jnp.einsum("htc,htsc,hsc->hts", query_matrix_rows, fade_upto, write_vector)
    query_key = jnp.einsum("htc,htsc,hsc->hts", query_matrix_rows, fade_upto, key_matrix_rows)
    identity = jnp.broadcast_to(jnp.eye(length, dtype=jnp.float32), erase_write.shape)
    inverse = jax.scipy.linalg.solve_triangular(
        identity - erase_write, identity, lower=True, unit_diagonal=True
    )
    to_end = jnp.exp(cumulative[:, -1:, :] - cumulative)
    return (
        inverse,
        erase_key,
        query_write,
        query_key,
        jnp.exp(before_decay) * erase_vector,
        jnp.exp(cumulative) * query_matrix_rows,
        to_end * write_vector,
        to_end * key_matrix_rows,
        jnp.exp(cumulative[:, -1, :]),
    )


def advance_block(carried, tables, block_values, with_output):
    (
        inverse,
        erase_key,
        query_write,
        query_key,
        start_erase,
        start_query,
        end_write,
        end_key,
        end_fade,
    ) = tables
    right_side = jnp.einsum("htk,hpk->htp", start_erase, carried) + jnp.einsum(
        "hts,hsp->htp", erase_key, block_values
    )
    held = jnp.einsum("hts,hsp->htp", inverse, right_side)
    next_state = (
        carried * end_fade[:, None, :]
        + jnp.einsum("htp,htk->hpk", held, end_write)
        + jnp.einsum("htp,htk->hpk", block_values, end_key)
    )
    if not with_output:
        return (next_state, None)
    output = (
        jnp.einsum("htk,hpk->htp", start_query, carried)
        + jnp.einsum("hts,hsp->htp", query_write, held)
        + jnp.einsum("hts,hsp->htp", query_key, block_values)
    )
    return (next_state, output)


def chain(earlier, later):
    product = jnp.einsum("hij,hjk->hik", earlier[0], later[0])
    added = jnp.einsum("hij,hjk->hik", earlier[1], later[0]) + later[1]
    return (product, added)


def slot_positions(route_block, experts):
    flat_ids = route_block.reshape(-1)
    onehot = (flat_ids[:, None] == jnp.arange(experts, dtype=jnp.int32)[None, :]).astype(jnp.int32)
    earlier_count = jnp.cumsum(onehot, axis=0) - onehot
    return jnp.sum(earlier_count * onehot, axis=1).reshape(route_block.shape)


def per_device(
    mixer_input,
    mixer_gain,
    query_matrix,
    key_matrix,
    value_matrix,
    decay_down_factor,
    decay_up_factor,
    decay_bias_base,
    decay_shift,
    decay_spike,
    correction_rate_down,
    correction_rate_up,
    correction_rate_base,
    head_norm_gain,
    output_weight,
    feedforward_input,
    feedforward_gain,
    routed_expert_index,
    routed_expert_weight,
    expert_gate_weight,
    expert_up_weight,
    expert_down_weight,
    shared_gate_weight,
    shared_up_weight,
    shared_down_weight,
):
    tp_size = lax.axis_size("tp")
    ep_size = lax.axis_size(EP)
    normed_first = rms_rows(mixer_input, mixer_gain)
    (
        query_matrix_rows,
        key_matrix_rows,
        value_matrix_rows,
        erase_vector,
        write_vector,
        logarithm_decay,
    ) = mixer_channel_rows(
        normed_first,
        query_matrix,
        key_matrix,
        value_matrix,
        decay_down_factor,
        decay_up_factor,
        decay_bias_base,
        decay_shift,
        decay_spike,
        correction_rate_down,
        correction_rate_up,
        correction_rate_base,
    )
    row_count, head_count, head_size = query_matrix_rows.shape
    block_count = row_count // SPAN

    def to_blocks(matrix):
        return matrix.reshape(block_count, SPAN, head_count, head_size).transpose(0, 2, 1, 3)

    tables = lax.map(
        lambda block_items: block_tables(*block_items),
        (
            to_blocks(query_matrix_rows),
            to_blocks(key_matrix_rows),
            to_blocks(erase_vector),
            to_blocks(write_vector),
            to_blocks(logarithm_decay),
        ),
    )
    value_blocks = to_blocks(value_matrix_rows)
    identity = jnp.broadcast_to(
        jnp.eye(head_size, dtype=jnp.float32), (head_count, head_size, head_size)
    )
    zero_state = jnp.zeros((head_count, head_size, head_size), jnp.float32)

    def state_only(carried, block_items):
        block_table, block_values = block_items
        widened = jnp.concatenate([block_values, jnp.zeros_like(block_values)], axis=2)
        return (advance_block(carried, block_table, widened, False)[0], None)

    final_state, _ = lax.scan(
        state_only, jnp.concatenate([zero_state, identity], axis=1), (tables, value_blocks)
    )
    _, incoming = prefix_by_axis(
        (final_state[:, head_size:], final_state[:, :head_size]), EP, chain, (identity, zero_state)
    )

    def with_output(carried, block_items):
        block_table, block_values = block_items
        return advance_block(carried, block_table, block_values, True)

    _, head_out = lax.scan(with_output, incoming, (tables, value_blocks))
    head_out = head_out.transpose(0, 2, 1, 3).reshape(row_count, head_count, head_size)
    mixed_rows = head_norm(head_out, head_norm_gain)
    mixed_a = summed_on_arrival(
        jnp.dot(mixed_rows, output_weight, preferred_element_type=jnp.float32).astype(jnp.bfloat16),
        "tp",
        0,
    ).astype(jnp.bfloat16)
    own_count = feedforward_input.shape[0]
    local_count = expert_gate_weight.shape[0]
    experts = local_count * ep_size
    capacity = max(2, 3 * own_count * TOP // (2 * experts))
    normed_own = rms_rows(feedforward_input, feedforward_gain)
    model_width = normed_own.shape[1]
    group_rows = gather_directly(normed_own, "tp", 0)
    own_ids = lax.dynamic_slice_in_dim(
        routed_expert_index, lax.axis_index("tp") * own_count, own_count, 0
    )
    own_positions = slot_positions(own_ids, experts)
    zero_row = jnp.zeros((1, model_width), jnp.bfloat16)
    slot_index = own_ids * capacity + own_positions
    slot_table = jnp.full((experts * capacity,), own_count, jnp.int32)
    slot_table = slot_table.at[slot_index.reshape(-1)].set(
        jnp.broadcast_to(jnp.arange(own_count, dtype=jnp.int32)[:, None], slot_index.shape).reshape(
            -1
        )
    )
    padded = jnp.concatenate([normed_own, zero_row], axis=0)
    outgoing = padded[slot_table].reshape(experts, capacity, model_width)
    received = lax.all_to_all(outgoing, EP, split_axis=0, concat_axis=0, tiled=True)
    arrived = lax.all_gather(received[None], "tp", axis=0, tiled=True)
    arrived = arrived.reshape(tp_size, ep_size, local_count, capacity, model_width)
    gate_out = jnp.einsum(
        "tgjcd,jdf->tgjcf", arrived, expert_gate_weight, preferred_element_type=jnp.float32
    )
    up_out = jnp.einsum(
        "tgjcd,jdf->tgjcf", arrived, expert_up_weight, preferred_element_type=jnp.float32
    )
    hidden = (jax.nn.silu(gate_out) * up_out).astype(jnp.bfloat16)
    shared_hidden = (
        jax.nn.silu(jnp.dot(group_rows, shared_gate_weight, preferred_element_type=jnp.float32))
        * jnp.dot(group_rows, shared_up_weight, preferred_element_type=jnp.float32)
    ).astype(jnp.bfloat16)
    shared_hidden = shared_hidden.reshape(tp_size, own_count, -1)
    routed_rows = ep_size * local_count * capacity
    block_rows = routed_rows + own_count
    block_total = lax.axis_size("tp") * block_rows // block_rows
    routed_part = jnp.einsum(
        "tgjcf,jfd->tgjcd", hidden, expert_down_weight, preferred_element_type=jnp.float32
    )
    shared_part = jnp.einsum(
        "tnf,fd->tnd", shared_hidden, shared_down_weight, preferred_element_type=jnp.float32
    )
    joined = jnp.concatenate(
        [routed_part.reshape(block_total, routed_rows, model_width), shared_part], axis=1
    )
    summed = lax.psum_scatter(
        joined.reshape(lax.axis_size("tp") * block_rows, model_width).astype(jnp.bfloat16),
        "tp",
        scatter_dimension=0,
        tiled=True,
    ).astype(jnp.float32)
    expert_out = (
        summed[:routed_rows]
        .astype(jnp.bfloat16)
        .reshape(ep_size, local_count * capacity, model_width)
    )
    returned = lax.all_to_all(expert_out, EP, split_axis=0, concat_axis=0, tiled=True).reshape(
        experts * capacity, model_width
    )
    picked = returned[own_ids * capacity + own_positions]
    routed = jnp.einsum("rk,rkd->rd", routed_expert_weight, picked.astype(jnp.float32))
    mixed_b = (routed + summed[routed_rows:]).astype(jnp.bfloat16)
    return (mixed_a, mixed_b)


def solution(mesh):
    split = Mesh(mesh.devices.reshape(8, 4, mesh.shape["tp"]), ("ep_0", "ep_1", "tp"))
    return jax.shard_map(
        per_device,
        mesh=split,
        in_specs=(
            P(EP, None),
            P(),
            P(None, "tp"),
            P(None, "tp"),
            P(None, "tp"),
            P(),
            P(None, "tp"),
            P("tp"),
            P(EP, "tp"),
            P(EP, "tp"),
            P(),
            P(None, "tp"),
            P("tp"),
            P("tp"),
            P("tp", None),
            P(EP_TP, None),
            P(),
            P(EP, None),
            P(EP_TP, None),
            P(EP, None, "tp"),
            P(EP, None, "tp"),
            P(EP, "tp", None),
            P(None, "tp"),
            P(None, "tp"),
            P("tp", None),
        ),
        out_specs=(P(EP_TP, None), P(EP_TP, None)),
        check_vma=False,
    )
```

profile of v0, /device:TPU:1, one launch (start us, length us, event | category | flops | bytes accessed | tf_op | source)
XLA Modules:
  0.0 303.2 jit_solution(10269002091156611758)
XLA Ops:
  11.0 1.0 fusion.156
  12.1 1.0 fusion.158
  13.8 0.9 gather_fusion
  14.7 1.1 reshape.255
  15.9 11.9 %all-to-all-start.1 = ((bf16[64,2,2048]{2,1,0:T(2,128)(2,1)}), bf16[64,2,2048]{2,1,0:T(2,128)(2,1)S(1)}, u32[]{:S(2)}, u32[]{:S(2)}) async-start(bf16[64,2,2048]{2,1,0:T(2,128)(2,1)} %reshape.255), calls=%async_computation.1 | async-start | bytes 1048576 | tf_op jit(solution)/shard_map/all_to_all | solution.py:337
  28.8 1.6 fusion.260
  32.3 1.6 fusion.250
  35.6 1.2 fusion.160
  36.8 67.5 %while.51 = (s32[]{:T(128)}, bf16[4,4,32,32]{3,2,1,0:T(8,128)(2,1)}, bf16[4,4,32,32]{3,2,1,0:T(8,128)(2,1)}, bf16[4,4,32,32]{3,2,1,0:T(8,128)(2,1)}, bf16[4,4,32...) while((s32[]{:T(128)}, ...), condition=%wide.region_4.5_spmd.clone, body=%wide.region_2.4_spmd.sunk.clone | while | flops 7146530 | bytes 3328645 | solution.py:276
  38.2 0.9 fusion.414
  39.2 0.9 fusion.413
  40.2 0.9 fusion.412
  41.2 0.9 fusion.409
  42.3 9.8 %custom-call.16 = f32[4,1,32,32]{2,3,1,0:T(8,128)S(1)} custom-call(f32[4,1,32,32]{3,2,1,0:T(8,128)S(1)} %add_bitcast_fusion.3), custom_call_target="InvertDiagBlocksLowerTriangular" | custom-call | tf_op jit(solution)/shard_map/while/body/eval_jaxpr/jit(_solve_triangular)/vmap()/triangular_solve | solution.py:158
  52.5 1.3 constant_dynamic-update-slice_fusion.12
  55.1 0.9 fusion.414
  56.0 0.9 fusion.413
  57.1 0.9 fusion.412
  58.1 0.9 fusion.409
  59.1 9.8 %custom-call.16 = f32[4,1,32,32]{2,3,1,0:T(8,128)S(1)} custom-call(f32[4,1,32,32]{3,2,1,0:T(8,128)S(1)} %add_bitcast_fusion.3), custom_call_target="InvertDiagBlocksLowerTriangular" | custom-call | tf_op jit(solution)/shard_map/while/body/eval_jaxpr/jit(_solve_triangular)/vmap()/triangular_solve | solution.py:158
  69.3 1.3 constant_dynamic-update-slice_fusion.12
  72.0 0.9 fusion.414
  72.9 0.9 fusion.413
  73.9 0.9 fusion.412
  74.9 0.9 fusion.409
  76.0 9.8 %custom-call.16 = f32[4,1,32,32]{2,3,1,0:T(8,128)S(1)} custom-call(f32[4,1,32,32]{3,2,1,0:T(8,128)S(1)} %add_bitcast_fusion.3), custom_call_target="InvertDiagBlocksLowerTriangular" | custom-call | tf_op jit(solution)/shard_map/while/body/eval_jaxpr/jit(_solve_triangular)/vmap()/triangular_solve | solution.py:158
  86.2 1.3 constant_dynamic-update-slice_fusion.12
  88.8 0.9 fusion.414
  89.7 0.9 fusion.413
  90.8 0.9 fusion.412
  92.8 9.8 %custom-call.16 = f32[4,1,32,32]{2,3,1,0:T(8,128)S(1)} custom-call(f32[4,1,32,32]{3,2,1,0:T(8,128)S(1)} %add_bitcast_fusion.3), custom_call_target="InvertDiagBlocksLowerTriangular" | custom-call | tf_op jit(solution)/shard_map/while/body/eval_jaxpr/jit(_solve_triangular)/vmap()/triangular_solve | solution.py:158
  103.0 1.3 constant_dynamic-update-slice_fusion.12
  104.3 1.8 fusion.248
  107.1 1.1 broadcast_in_dim.116
  108.2 5.4 %all-to-all-start.2 = ((bf16[8,32,2048]{2,1,0:T(8,128)(2,1)}), bf16[8,32,2048]{2,1,0:T(8,128)(2,1)S(1)}, u32[]{:S(2)}, u32[]{:S(2)}) async-start(bf16[8,32,2048]{2,1,0:T(8,128)(2,1)} %broadcast_in_dim.116), calls=%async_computation.2 | async-start | bytes 2097152 | tf_op jit(solution)/shard_map/all_to_all | solution.py:59
  114.4 6.5 %while.52 = (s32[]{:T(128)}, f32[4,128,64]{1,2,0:T(8,128)S(1)}, f32[4,4,64]{2,1,0:T(4,128)S(1)}, bf16[4,4,32,32]{3,2,1,0:T(8,128)(2,1)}, bf16[4,4,32,64]{3,2,1,0...) while((s32[]{:T(128)}, f32[4,128,64]{1,2,0:T(8,128)S(1)}, ...), condition=%wide.region_6.7_spmd.clone, body=%wide.region_5.6_spmd.sunk.clone | while | flops 8519682 | bytes 1102961 | solution.py:297
  114.6 1.0 fusion.425
  116.2 1.0 fusion.425
  117.9 1.0 fusion.425
  119.5 1.0 fusion.425
  121.1 10.3 %all-gather = bf16[16,64,64]{2,1,0:T(8,128)(2,1)S(1)} all-gather(bf16[4,64,64]{2,1,0:T(8,128)(2,1)S(1)} %get-tuple-element.351), channel_id=2, replica_groups=mesh['ep_0'=8,'ep_1'=4,'tp'=8] {'ep_1'}, dimensions={0}, use_global_device_ids=true | all-gather | bytes 163840 | tf_op jit(solution)/shard_map/all_gather | solution.py:31
  131.4 10.6 %all-gather.2 = bf16[16,64,64]{2,1,0:T(8,128)(2,1)S(1)} all-gather(bf16[4,64,64]{2,1,0:T(8,128)(2,1)S(1)} %get-tuple-element.352), channel_id=4, replica_groups=mesh['ep_0'=8,'ep_1'=4,'tp'=8] {'ep_1'}, dimensions={0}, use_global_device_ids=true | all-gather | bytes 163840 | tf_op jit(solution)/shard_map/all_gather | solution.py:31
  144.3 21.4 %all-gather.1 = bf16[32,64,64]{2,1,0:T(8,128)(2,1)S(1)} all-gather(bf16[4,64,64]{2,1,0:T(8,128)(2,1)S(1)} %fusion.227), channel_id=3, replica_groups=mesh['ep_0'=8,'ep_1'=4,'tp'=8] {'ep_0'}, dimensions={0}, use_global_device_ids=true | all-gather | bytes 294912 | tf_op jit(solution)/shard_map/all_gather | solution.py:31
  167.4 1.5 fusion.261
  169.0 1.5 fusion.141
  171.5 6.2 %fusion.116 = f32[8,32,2,2,128]{4,1,3,0,2:T(8,128)} fusion(bf16[8,32,2,2,2048]{4,3,2,1,0:T(2,128)(2,1)} %bitcast.403, bf16[2,2048,128]{2,1,0:T(8,128)(2,1)} %param.50), kind=kOutput, calls=%fused_computation.151 | convolution fusion | flops 536870912 | bytes 5767168 | tf_op jit(solution)/shard_map/tgjcd,jdf->tgjcf/dot_general | solution.py:340
  177.6 8.6 %convert_bitcast_fusion = bf16[8,32,2,2,2048]{4,1,3,0,2:T(8,128)(2,1)} fusion(bf16[8,32,2,2,2048]{4,3,2,1,0:T(2,128)(2,1)} %bitcast.404, bf16[2,128,2048]{2,1,0:T(8,128)(2,1)S(1)} %copy-done, bf16[2,2048,128]{2,1,0:T(8,128)(2,1)} %param.51, f32[8,32,2,2,128]{4,1,3,0,2:T(8,128)} %fusion.116), kind=kOutput, calls=%fused_computation.142 | convolution fusion | flops 1076625408 | bytes 11010048 | tf_op jit(solution)/shard_map/tgjcf,jfd->tgjcd/dot_general | solution.py:355
  186.2 4.5 %copy.96 = bf16[8,32,2,2,2048]{4,0,3,2,1:T(8,128)(2,1)S(1)} copy(bf16[8,32,2,2,2048]{4,1,3,0,2:T(8,128)(2,1)} %convert_bitcast_fusion) | data formatting | bytes 8388608 | tf_op jit(solution)/shard_map/tgjcf,jfd->tgjcd/transpose | solution.py:355
  191.2 5.4 %copy.98 = bf16[8,160,2048]{2,1,0:T(8,128)(2,1)} copy(bf16[8,160,2048]{2,0,1:T(8,128)(2,1)S(1)} %pad_maximum_fusion) | data formatting | bytes 10485760 | tf_op jit(solution)/shard_map/concatenate | solution.py:361
  196.7 19.0 %all-gather.3 = bf16[32,64,64]{2,1,0:T(8,128)(2,1)S(1)} all-gather(bf16[4,64,64]{2,1,0:T(8,128)(2,1)S(1)} %convolution_add_fusion.15), channel_id=5, replica_groups=mesh['ep_0'=8,'ep_1'=4,'tp'=8] {'ep_0'}, dimensions={0}, use_global_device_ids=true | all-gather | bytes 294912 | tf_op jit(solution)/shard_map/all_gather | solution.py:31
  218.9 1.3 fusion.132
  220.2 17.3 %while.53 = (s32[]{:T(128)}, f32[4,64,64]{2,1,0:T(8,128)S(1)}, f32[4,4,32,64]{3,2,1,0:T(8,128)S(1)}, f32[4,4,64]{2,1,0:T(4,128)S(1)}, bf16[4,4,32,32]{3,2,1,0:T(...) while((s32[]{:T(128)}, f32[4,64,64]{2,1,0:T(8,128)S(1)}, ...), condition=%wide.region_8.9_spmd.clone, body=%wide.region_7.8_spmd.sunk.clone | while | flops 6373378 | bytes 1352841 | solution.py:308
  220.3 1.0 fusion.442
  224.6 1.0 fusion.442
  229.0 1.0 fusion.442
  233.3 1.0 fusion.442
  238.8 1.1 convolution_convert_fusion.1
  239.9 20.8 %all-to-all-start = ((bf16[8,16,2048]{2,1,0:T(8,128)(2,1)}), bf16[8,16,2048]{2,1,0:T(8,128)(2,1)S(1)}, u32[]{:S(2)}, u32[]{:S(2)}) async-start(bf16[8,16,2048]{2,1,0:T(8,128)(2,1)} %bitcast.60), calls=%async_computation | async-start | bytes 1048576 | tf_op jit(solution)/shard_map/all_to_all | solution.py:53
  260.7 1.1 slice.184
  261.8 1.0 reshape.260
  262.8 7.3 %all-to-all-done = bf16[8,16,2048]{2,1,0:T(8,128)(2,1)S(1)} async-done(((bf16[8,16,2048]{2,1,0:T(8,128)(2,1)}), bf16[8,16,2048]{2,1,0:T(8,128)(2,1)S(1)}, u32[]{:S(2)}, u32[]{:S(2)}) %all-to-all-start) | async-done | bytes 524320 | tf_op jit(solution)/shard_map/all_to_all | solution.py:53
  270.1 7.8 %all-to-all-start.3 = ((bf16[32,4,2048]{2,1,0:T(4,128)(2,1)}), bf16[32,4,2048]{2,1,0:T(4,128)(2,1)S(1)}, u32[]{:S(2)}, u32[]{:S(2)}) async-start(bf16[32,4,2048]{2,1,0:T(4,128)(2,1)} %reshape.260), calls=%async_computation.4 | async-start | bytes 1048576 | tf_op jit(solution)/shard_map/all_to_all | solution.py:375
  278.8 14.4 %all-to-all-done.3 = bf16[32,4,2048]{2,1,0:T(4,128)(2,1)S(1)} async-done(((bf16[32,4,2048]{2,1,0:T(4,128)(2,1)}), bf16[32,4,2048]{2,1,0:T(4,128)(2,1)S(1)}, u32[]{:S(2)}, u32[]{:S(2)}) %all-to-all-start.3) | async-done | bytes 524320 | tf_op jit(solution)/shard_map/all_to_all | solution.py:375
  294.7 1.7 fusion.159
  (354 shorter events, 46.8 us)
Async XLA Ops:
  7.2 170.5 %copy-start = (bf16[2,128,2048]{2,1,0:T(8,128)(2,1)S(1)}, bf16[2,128,2048]{2,1,0:T(8,128)(2,1)}, u32[]{:S(2)}) copy-start(bf16[2,128,2048]{2,1,0:T(8,128)(2,1)} %param.52) | copy-start | bytes 3145732
  14.7 13.8 %copy-start.38 = (bf16[2048]{0:T(1024)(128)(2,1)S(1)}, bf16[2048]{0:T(1024)(128)(2,1)}, u32[]{:S(2)}) copy-start(bf16[2048]{0:T(1024)(128)(2,1)} %param.32) | copy-start | bytes 12292
  14.7 13.8 %copy-start.12 = (bf16[128,2048]{1,0:T(8,128)(2,1)S(1)}, bf16[128,2048]{1,0:T(8,128)(2,1)}, u32[]{:S(2)}) copy-start(bf16[128,2048]{1,0:T(8,128)(2,1)} %param.31) | copy-start | bytes 1572868
  15.9 91.2 %all-to-all-start.1 = ((bf16[64,2,2048]{2,1,0:T(2,128)(2,1)}), bf16[64,2,2048]{2,1,0:T(2,128)(2,1)S(1)}, u32[]{:S(2)}, u32[]{:S(2)}) async-start(bf16[64,2,2048]{2,1,0:T(2,128)(2,1)} %reshape.255), calls=%async_computation.1 | async-start | bytes 1048576 | tf_op jit(solution)/shard_map/all_to_all | solution.py:337
  27.7 3.0 copy-start.40
  27.7 3.0 copy-start.44
  27.7 3.0 copy-start.46
  28.5 6.2 %copy-start.37 = (f32[2048]{0:T(1024)}, f32[2048]{0:T(1024)S(1)}, u32[]{:S(2)}) copy-start(f32[2048]{0:T(1024)S(1)} %convert_element_type.164) | copy-start | bytes 24580
  28.8 6.0 %copy-start.49 = (f32[128]{0:T(128)}, f32[128]{0:T(128)S(1)}, u32[]{:S(2)}) copy-start(f32[128]{0:T(128)S(1)} %add_rsqrt_fusion.3) | copy-start | bytes 1540
  30.8 4.0 %copy-start.42 = (f32[128,256]{1,0:T(8,128)S(1)}, f32[128,256]{1,0:T(8,128)}, u32[]{:S(2)}) copy-start(f32[128,256]{1,0:T(8,128)} %param.40) | copy-start | bytes 393220
  30.8 4.0 %copy-start.43 = (f32[128,256]{1,0:T(8,128)S(1)}, f32[128,256]{1,0:T(8,128)}, u32[]{:S(2)}) copy-start(f32[128,256]{1,0:T(8,128)} %param.39) | copy-start | bytes 393220
  30.8 4.0 %copy-start.45 = (bf16[64,256]{1,0:T(8,128)(2,1)S(1)}, bf16[64,256]{1,0:T(8,128)(2,1)}, u32[]{:S(2)}) copy-start(bf16[64,256]{1,0:T(8,128)(2,1)} %param.37) | copy-start | bytes 98308
  30.8 4.0 %copy-start.47 = (f32[256]{0:T(256)S(1)}, f32[256]{0:T(256)}, u32[]{:S(2)}) copy-start(f32[256]{0:T(256)} %param.38) | copy-start | bytes 3076
  31.4 3.3 %copy-start.41 = (bf16[2048,64]{0,1:T(8,128)(2,1)S(1)}, bf16[2048,64]{0,1:T(8,128)(2,1)}, u32[]{:S(2)}) copy-start(bf16[2048,64]{0,1:T(8,128)(2,1)} %param.36) | copy-start | bytes 786436
  38.2 1.9 copy-start.30
  38.2 1.9 copy-start.32
  40.2 2.0 copy-start.31
  40.2 2.0 copy-start.33
  41.1 11.0 %copy-start.5 = (bf16[4,4,32,32]{3,2,1,0:T(8,128)(2,1)S(1)}, bf16[4,4,32,32]{3,2,1,0:T(8,128)(2,1)}, u32[]{:S(2)}) copy-start(bf16[4,4,32,32]{3,2,1,0:T(8,128)(2,1)} %get-tuple-element.720) | copy-start | bytes 98308 | tf_op jit(solution)/shard_map/while
  52.4 1.3 copy-start.6
  55.1 1.9 copy-start.30
  55.1 1.9 copy-start.32
  57.0 2.0 copy-start.31
  57.0 2.0 copy-start.33
  58.0 11.0 %copy-start.5 = (bf16[4,4,32,32]{3,2,1,0:T(8,128)(2,1)S(1)}, bf16[4,4,32,32]{3,2,1,0:T(8,128)(2,1)}, u32[]{:S(2)}) copy-start(bf16[4,4,32,32]{3,2,1,0:T(8,128)(2,1)} %get-tuple-element.720) | copy-start | bytes 98308 | tf_op jit(solution)/shard_map/while
  58.0 1.1 copy-start.8
  69.3 1.3 copy-start.6
  71.9 1.9 copy-start.30
  71.9 1.9 copy-start.32
  73.8 1.1 copy-start.7
  73.9 2.0 copy-start.31
  73.9 2.0 copy-start.33
  74.9 11.0 %copy-start.5 = (bf16[4,4,32,32]{3,2,1,0:T(8,128)(2,1)S(1)}, bf16[4,4,32,32]{3,2,1,0:T(8,128)(2,1)}, u32[]{:S(2)}) copy-start(bf16[4,4,32,32]{3,2,1,0:T(8,128)(2,1)} %get-tuple-element.720) | copy-start | bytes 98308 | tf_op jit(solution)/shard_map/while
  86.2 1.3 copy-start.6
  88.8 1.9 copy-start.30
  88.8 1.9 copy-start.32
  90.7 2.0 copy-start.31
  90.7 2.0 copy-start.33
  91.7 11.0 %copy-start.5 = (bf16[4,4,32,32]{3,2,1,0:T(8,128)(2,1)S(1)}, bf16[4,4,32,32]{3,2,1,0:T(8,128)(2,1)}, u32[]{:S(2)}) copy-start(bf16[4,4,32,32]{3,2,1,0:T(8,128)(2,1)} %get-tuple-element.720) | copy-start | bytes 98308 | tf_op jit(solution)/shard_map/while
  103.0 1.3 copy-start.6
  104.3 2.8 copy-start.3
  106.9 7.5 %copy-start.36 = (f32[4,4,64]{2,1,0:T(4,128)S(1)}, f32[4,4,64]{2,1,0:T(4,128)}, u32[]{:S(2)}) copy-start(f32[4,4,64]{2,1,0:T(4,128)} %get-tuple-element.779) | copy-start | bytes 12292
  107.1 6.6 %copy-start.1 = (bf16[64,2,2048]{2,1,0:T(2,128)(2,1)}, bf16[64,2,2048]{2,1,0:T(2,128)(2,1)S(1)}, u32[]{:S(2)}) copy-start(bf16[64,2,2048]{2,1,0:T(2,128)(2,1)S(1)} %all-to-all-done.1) | copy-start | bytes 1572868
  108.2 59.2 %all-to-all-start.2 = ((bf16[8,32,2048]{2,1,0:T(8,128)(2,1)}), bf16[8,32,2048]{2,1,0:T(8,128)(2,1)S(1)}, u32[]{:S(2)}, u32[]{:S(2)}) async-start(bf16[8,32,2048]{2,1,0:T(8,128)(2,1)} %broadcast_in_dim.116), calls=%async_computation.2 | async-start | bytes 2097152 | tf_op jit(solution)/shard_map/all_to_all | solution.py:59
  113.7 57.8 %all-gather.7.cloned.1.call-start = ((), (), s32[]{:S(2)}) async-start(), calls=%async_computation.6 | async-start | bytes 4718592 | tf_op jit(solution)/shard_map/all_gather | solution.py:338
  114.4 146.3 %reduce-scatter.2.cloned.1.call-start = ((), (), s32[]{:S(2)}) async-start(), calls=%async_computation.5 | async-start | bytes 5898240 | tf_op jit(solution)/shard_map/reduce_scatter | solution.py:364
  114.4 27.5 %copy-start.14 = (f32[64,64]{1,0:T(8,128)S(1)}, f32[64,64]{1,0:T(8,128)}, u32[]{:S(2)}) copy-start(f32[64,64]{1,0:T(8,128)} %copy-done.13) | copy-start | bytes 49156
  144.3 21.6 %copy-start.20 = (bf16[4,64,64]{2,1,0:T(8,128)(2,1)}, bf16[4,64,64]{2,1,0:T(8,128)(2,1)S(1)}, u32[]{:S(2)}) copy-start(bf16[4,64,64]{2,1,0:T(8,128)(2,1)S(1)} %fusion.227) | copy-start | bytes 98308
  167.4 3.0 copy-start.11
  196.6 21.4 %copy-start.10 = (bf16[4,64,64]{2,1,0:T(8,128)(2,1)S(1)}, bf16[4,64,64]{2,1,0:T(8,128)(2,1)}, u32[]{:S(2)}) copy-start(bf16[4,64,64]{2,1,0:T(8,128)(2,1)} %copy-done.9) | copy-start | bytes 98308
  196.6 21.4 %copy-start.15 = (f32[64,64]{1,0:T(8,128)S(1)}, f32[64,64]{1,0:T(8,128)}, u32[]{:S(2)}) copy-start(f32[64,64]{1,0:T(8,128)} %copy-done.13) | copy-start | bytes 49156
  196.6 21.4 %copy-start.25 = (bf16[4,64,64]{2,1,0:T(8,128)(2,1)S(1)}, bf16[4,64,64]{2,1,0:T(8,128)(2,1)}, u32[]{:S(2)}) copy-start(bf16[4,64,64]{2,1,0:T(8,128)(2,1)} %copy-done.24) | copy-start | bytes 98308
  196.7 22.2 %copy-start.17 = (bf16[4,64,64]{2,1,0:T(8,128)(2,1)S(1)}, bf16[4,64,64]{2,1,0:T(8,128)(2,1)}, u32[]{:S(2)}) copy-start(bf16[4,64,64]{2,1,0:T(8,128)(2,1)} %copy-done.16) | copy-start | bytes 98308
  196.7 22.2 %copy-start.19 = (bf16[4,64,64]{2,1,0:T(8,128)(2,1)S(1)}, bf16[4,64,64]{2,1,0:T(8,128)(2,1)}, u32[]{:S(2)}) copy-start(bf16[4,64,64]{2,1,0:T(8,128)(2,1)} %copy-done.18) | copy-start | bytes 98308
  196.7 22.2 %copy-start.21 = (bf16[4,64,64]{2,1,0:T(8,128)(2,1)S(1)}, bf16[4,64,64]{2,1,0:T(8,128)(2,1)}, u32[]{:S(2)}) copy-start(bf16[4,64,64]{2,1,0:T(8,128)(2,1)} %copy-done.20) | copy-start | bytes 98308
  196.7 22.2 %copy-start.23 = (bf16[4,64,64]{2,1,0:T(8,128)(2,1)S(1)}, bf16[4,64,64]{2,1,0:T(8,128)(2,1)}, u32[]{:S(2)}) copy-start(bf16[4,64,64]{2,1,0:T(8,128)(2,1)} %copy-done.22) | copy-start | bytes 98308
  216.8 1.2 copy-start.26
  216.9 1.1 copy-start.27
  237.5 1.3 copy-start.48
  237.5 1.3 copy-start.4
  239.9 37.9 %copy-start.34 = (s32[32,2]{1,0:T(8,128)S(1)}, s32[32,2]{1,0:T(8,128)}, u32[]{:S(2)}) copy-start(s32[32,2]{1,0:T(8,128)} %get-tuple-element.322) | copy-start | bytes 772
  239.9 38.1 %copy-start.39 = (f32[32,2]{0,1:T(2,128)S(1)}, f32[32,2]{0,1:T(2,128)}, u32[]{:S(2)}) copy-start(f32[32,2]{0,1:T(2,128)} %param.49) | copy-start | bytes 772
  239.9 30.2 %all-to-all-start = ((bf16[8,16,2048]{2,1,0:T(8,128)(2,1)}), bf16[8,16,2048]{2,1,0:T(8,128)(2,1)S(1)}, u32[]{:S(2)}, u32[]{:S(2)}) async-start(bf16[8,16,2048]{2,1,0:T(8,128)(2,1)} %bitcast.60), calls=%async_computation | async-start | bytes 1048576 | tf_op jit(solution)/shard_map/all_to_all | solution.py:53
  270.1 23.1 %all-to-all-start.3 = ((bf16[32,4,2048]{2,1,0:T(4,128)(2,1)}), bf16[32,4,2048]{2,1,0:T(4,128)(2,1)S(1)}, u32[]{:S(2)}, u32[]{:S(2)}) async-start(bf16[32,4,2048]{2,1,0:T(4,128)(2,1)} %reshape.260), calls=%async_computation.4 | async-start | bytes 1048576 | tf_op jit(solution)/shard_map/all_to_all | solution.py:375
  (16 other events, 13.0 us)
Sparse Core Ops, SparseCore 0:
  116.3 36.1 all-gather.6
  196.7 49.1 reduce-scatter.1
where the time goes:
time: 307 us; the launch traced here: 303 us
  matrix products  70.6 us (23%)
  blocking collectives  61.3 us (20%)
  other arithmetic  51.3 us (17%)
  starting transfers between devices  45.9 us (15%)
  local copies, waits for them, and re-layouts  35.8 us (12%)
  waiting for transfers between devices  22.5 us (7%)
  between operations  15 us (5%)
    all_gather x4, blocking collectives, prefix_by_axis(): lax.all_gather(part.astype(kind), axis)  61.3 us
    another operation x20, other arithmetic, block_tables(): jax.scipy.linalg.solve_triangular(identity - erase_write, identity, lower...  39.8 us
    all_to_all x1, starting transfers between devices, summed_on_arrival(): lax.all_to_all(blocks, axis, split_axis=0, concat_axis=0, tiled=True)  20.8 us
    all_to_all x1, waiting for transfers between devices, per_device(): lax.all_to_all(expert_out, EP, split_axis=0, concat_axis=0, tiled=True)  14.4 us
    all_to_all x1, starting transfers between devices, per_device(): lax.all_to_all(outgoing, EP, split_axis=0, concat_axis=0, tiled=True)  11.9 us
    dot_general x1, matrix products, per_device(): jnp.einsum('tgjcf,jfd->tgjcd', hidden, expert_down_weight, preferred_elem...  8.61 us
    dot_general x8, matrix products, advance_block(): held = jnp.einsum('hts,hsp->htp', inverse, right_side)  8.26 us
    all_to_all x1, starting transfers between devices, per_device(): lax.all_to_all(expert_out, EP, split_axis=0, concat_axis=0, tiled=True)  7.77 us
  transfers between devices with their start and end apart: 6, of which 2 were waited for; matrix products, arithmetic and copies ran while one was open for 38% of the time, Pallas kernels for 0%

commit v1 on v0

v1 whole, which is shorter than its diff:
```python
import jax
import jax.numpy as jnp
from jax import lax
from jax.experimental import pallas as pl
from jax.experimental.pallas import tpu as pltpu
from jax.sharding import Mesh
from jax.sharding import PartitionSpec as P

MESH = pl.DeviceIdType.MESH
BF, F32 = jnp.bfloat16, jnp.float32
norm_eps = 1e-06
group_eps = 0.00064
unit_eps = 1e-06
ROOT = 0.6065306597126334

HEADS = 4
HEAD = 64
SPAN = 32
ROWS = 128
TOK = 32
CHUNKS = 4
HALF = 1024
DZ = (0, 1, 7, 2, 6, 3, 5, 4)


def iota(shape, dim):
    return lax.broadcasted_iota(jnp.int32, shape, dim)


def dot(a, b, dims=((1,), (0,))):
    return lax.dot_general(a.astype(BF), b.astype(BF), (dims, ((), ())), preferred_element_type=F32)


def split(a):
    high = a.astype(BF)
    return high, (a - high.astype(F32)).astype(BF)


def dot3(a, b):
    ah, al = split(a)
    bh, bl = split(b)
    return dot(ah, bh) + (dot(ah, bl) + dot(al, bh))


def dot_exact_left(a, b):
    bh, rest = b.astype(BF), None
    rest = b - bh.astype(F32)
    bm = rest.astype(BF)
    bl = (rest - bm.astype(F32)).astype(BF)
    return dot(a, bh) + (dot(a, bm) + dot(a, bl))


def dot_exact_right(a, b):
    ah = a.astype(BF)
    rest = a - ah.astype(F32)
    am = rest.astype(BF)
    al = (rest - am.astype(F32)).astype(BF)
    return dot(ah, b) + (dot(am, b) + dot(al, b))


def sigmoid(u):
    e = jnp.exp(-jnp.abs(u))
    return jnp.where(u >= 0, 1.0, e) / (1.0 + e)


def rms(values, gain):
    values = values.astype(F32)
    scaled = values * lax.rsqrt(jnp.mean(values * values, axis=-1, keepdims=True) + norm_eps)
    return (scaled * gain.astype(F32)).astype(BF)


def ones_where(mask, kind=BF):
    return jnp.where(mask, 1.0, 0.0).astype(kind)


def compose(later, earlier):
    lane = iota(later.shape, 1)
    return dot3(later[:, :HEAD], earlier) + jnp.where(lane >= HEAD, later, 0.0)


def quarter_rows(matrix):
    return jnp.concatenate([matrix[:, 512 * q : 512 * (q + 1)] for q in range(4)], axis=0)


def quarter_lanes(matrix, rows):
    return jnp.concatenate([matrix[rows * q : rows * (q + 1)] for q in range(4)], axis=1)


def kernel(
    xa, gain_a, wq, wk, wv, decay_down, decay_up, decay_bias, decay_shift, decay_spike,
    rate_down, rate_up, rate_base, head_gain, w_out, xb, gain_b, ids, weights,
    e_gate, e_up, e_down, s_gate, s_up, s_down,
    out_a, out_b,
    v_xa, v_qkv, v_dd, v_rd, v_shift, v_spike, v_out, v_egu, v_ed, v_sgu, v_sd,
    tx, rx, rtx, rrx, X, Y, PR, Z, RA, RB, FA, FD, FB, FE, CA, CB,
    YA, PA, ZA, RAa, RBa, FAa, FDa, FBa, FEa, CAa, CBa,
    cmat, umat, mixed, atx, arx, ztx, zrx, btx, brx, sel_hi, sel_lo,
    lsem, tsem, rsem, ssend, srecv,
):
    z, x, y, c = (lax.axis_index(name) for name in ("z", "x", "y", "c"))
    yp, ym, cc = (y + 1) & 3, (y + 3) & 3, 1 - c
    used = [0]
    started = []

    local = {}

    def fetch(name, src, dst):
        copy = pltpu.make_async_copy(src, dst, lsem.at[len(local)])
        copy.start()
        local[name] = copy

    fetch("xa", xa, v_xa)
    fetch("wq", wq, v_qkv.at[:, 0:256])
    fetch("wk", wk, v_qkv.at[:, 256:512])
    fetch("wv", wv, v_qkv.at[:, 512:768])
    fetch("dd", decay_down, v_dd)
    fetch("rd", rate_down, v_rd)
    fetch("shift", decay_shift, v_shift)
    fetch("spike", decay_spike, v_spike)
    fetch("sg", s_gate, v_sgu.at[:, 0:128])
    fetch("su", s_up, v_sgu.at[:, 128:256])
    fetch("sd", s_down, v_sd)
    fetch("eg", e_gate, v_egu.at[:, :, 0:128])
    fetch("eu", e_up, v_egu.at[:, :, 128:256])
    fetch("ed", e_down, v_ed)
    fetch("out", w_out, v_out)

    def arrive(*names):
        for name in names:
            local[name].wait()

    barrier = pltpu.get_barrier_semaphore()

    def peer(place):
        return {"z": (z + DZ[place // 4]) & 7, "x": (x + place % 4) & 3}

    def source(place):
        return {"z": (z - DZ[place // 4]) & 7, "x": (x - place % 4) & 3}

    for place in range(1, 32):
        pl.semaphore_signal(barrier, inc=1, device_id=peer(place), device_id_type=MESH)
    for target in ({"y": yp}, {"y": ym}, {"c": cc}):
        pl.semaphore_signal(barrier, inc=1, device_id=target, device_id_type=MESH)

    def send(src, dst, target):
        n = used[0]
        used[0] += 1
        copy = pltpu.make_async_remote_copy(
            src_ref=src, dst_ref=dst, send_sem=ssend.at[n], recv_sem=srecv.at[n],
            device_id=target, device_id_type=MESH,
        )
        copy.start()
        started.append(copy)
        return copy

    normed_b = rms(xb[...], gain_b[...])
    mine = 32 * (2 * y + c)
    pick = ones_where(iota((256, 128), 0) == mine + (iota((256, 128), 1) & 31))
    own_ids = dot(ids[...].astype(F32), pick).astype(jnp.int32)
    expert = iota((128, 128), 0) >> 1
    first, second = own_ids[0:1] == expert, own_ids[1:2] == expert
    named = ones_where(first | second)
    lane, row = iota((128, 128), 1), iota((128, 128), 0)
    earlier = ones_where(((row >> 5) == (lane >> 5)) & (row < lane))
    count = dot(named, earlier)
    taken = (first | second) & (count == (row & 1).astype(F32))
    spread = ones_where((iota((32, 128), 1) & 31) == iota((32, 128), 0))
    w_tiled = dot_exact_right(weights[...], spread)
    slot_weight = jnp.where(taken, jnp.where(first, w_tiled[0:1], w_tiled[1:2]), 0.0)
    R, S = iota((512, 128), 0), iota((512, 128), 1)
    turn = R >> 6
    dz = jnp.where((turn & 1) == 1, (turn + 1) >> 1, (8 - (turn >> 1)) & 7)
    group = (((z + dz) & 7) << 2) + ((x + ((R >> 4) & 3)) & 3)
    place_of = ones_where(S == (group << 2) + (R & 3))
    own_quarter = ((R >> 2) & 3) == (S >> 5)
    chosen = jnp.where(own_quarter, dot(place_of, ones_where(taken)), 0.0)
    outgoing = dot(chosen, quarter_rows(normed_b)).astype(BF)
    tx[...] = outgoing.reshape(32, 16, 512)
    rx[0] = outgoing[0:16]
    X[4, 0, 0] = normed_b

    pl.semaphore_wait(barrier, 34)
    dispatched = []
    for place in range(1, 32):
        copy = pltpu.make_async_remote_copy(
            src_ref=tx.at[place], dst_ref=rx.at[place], send_sem=tsem.at[place],
            recv_sem=rsem.at[place], device_id=peer(place), device_id_type=MESH,
        )
        copy.start()
        dispatched.append(copy)

    gathers = {}

    def gather1(k):
        own = X.at[k, 0, 0]
        gathers[k] = [
            send(own, X.at[k, 0, 3], {"y": yp}),
            send(own, X.at[k, 0, 1], {"y": ym}),
            send(own, X.at[k, 1, 0], {"c": cc}),
        ]

    def gather2(k):
        held = gathers[k]
        held[0].wait_recv()
        left = X.at[k, 0, 3]
        held.append(send(left.at[:, 0:HALF], X.at[k, 0, 2, :, 0:HALF], {"y": yp}))
        held.append(send(left, X.at[k, 1, 3], {"c": cc}))
        held[1].wait_recv()
        right = X.at[k, 0, 1]
        held.append(send(right.at[:, HALF:], X.at[k, 0, 2, :, HALF:], {"y": ym}))
        held.append(send(right, X.at[k, 1, 1], {"c": cc}))

    def gather3(k):
        held = gathers[k]
        held[3].wait_recv()
        held[5].wait_recv()
        held.append(send(X.at[k, 0, 2], X.at[k, 1, 2], {"c": cc}))

    def gather4(k):
        held = gathers[k]
        for n in (2, 4, 6, 7):
            held[n].wait_recv()

    gather1(4)

    by_place = [jnp.where(own_quarter, dot(place_of, part), 0.0).astype(BF) for part in split(slot_weight)]
    sel_hi[...], sel_lo[...] = by_place

    def tile_row(a):
        return (((a >> 1) & 7) << 4) + ((a >> 5) << 2) + (((a >> 4) & 1) << 1) + (a & 1)

    def unpack_matrix():
        return ones_where(lane == tile_row(row))

    def pack_matrix():
        return ones_where(row == tile_row(lane))

    def unpack(k):
        for place in range(8 * k, 8 * k + 8):
            if place:
                dispatched[place - 1].wait_recv()
        tiles = rx[8 * k : 8 * k + 8].reshape(128, 512)
        stacked = dot(unpack_matrix(), tiles).astype(BF)
        X[k, 0, 0] = quarter_lanes(stacked, 32)

    def hidden_of(rows, gate_up):
        both = dot(rows, gate_up)
        gate = both[:, 0:128]
        return (gate * sigmoid(gate) * both[:, 128:256]).astype(BF)

    def experts(k):
        for j in range(2):
            rows = X[k, :, :, 16 * j : 16 * j + 16, :].reshape(128, 2048)
            hidden = hidden_of(rows, v_egu[j])
            Y[k, :, :, 16 * j : 16 * j + 16, :] = dot(hidden, v_ed[j]).astype(BF).reshape(2, 4, 16, 2048)

    def shared_expert():
        rows = X[4].reshape(256, 2048)
        hidden = hidden_of(rows, v_sgu[...])
        Y[4] = dot(hidden, v_sd[...]).astype(BF).reshape(2, 4, 32, 2048)

    sums = {}

    def refs_of(k):
        if k == "a":
            return YA, PA, ZA, RAa, RBa, FAa, FDa, FBa, FEa, CAa, CBa
        return tuple(ref.at[k] for ref in (Y, PR, Z, RA, RB, FA, FD, FB, FE, CA, CB))

    def sum1(k):
        refs = refs_of(k)
        sums[k] = [send(refs[0].at[1], refs[1], {"c": cc})]

    def sum2(k):
        part, pair, total, ra, rb, fa, fd, fb, fe, ca, cb = refs_of(k)
        held = sums[k]
        held[0].wait_recv()
        total[...] = (part[0].astype(F32) + pair[...].astype(F32)).astype(BF)
        held.append(send(total.at[2, :, 0:HALF], ra, {"y": yp}))
        held.append(send(total.at[2, :, HALF:], rb, {"y": ym}))
        held.append(send(total.at[1, :, HALF:], fe, {"y": yp}))
        held.append(send(total.at[3, :, 0:HALF], fd, {"y": ym}))

    def sum3(k):
        part, pair, total, ra, rb, fa, fd, fb, fe, ca, cb = refs_of(k)
        held = sums[k]
        held[1].wait_recv()
        ca[...] = (total[1, :, 0:HALF].astype(F32) + ra[...].astype(F32)).astype(BF)
        held.append(send(ca, fa, {"y": yp}))
        held[2].wait_recv()
        cb[...] = (total[3, :, HALF:].astype(F32) + rb[...].astype(F32)).astype(BF)
        held.append(send(cb, fb, {"y": ym}))

    def sum4(k):
        part, pair, total, ra, rb, fa, fd, fb, fe, ca, cb = refs_of(k)
        for n in (3, 4, 5, 6):
            sums[k][n].wait_recv()
        low = total[0, :, 0:HALF].astype(F32) + (fa[...].astype(F32) + fd[...].astype(F32))
        high = total[0, :, HALF:].astype(F32) + (fb[...].astype(F32) + fe[...].astype(F32))
        return jnp.concatenate([low, high], axis=1)

    returned = []

    def give_back(k):
        stacked = quarter_rows(sum4(k).astype(BF))
        packed = dot(pack_matrix(), stacked).astype(BF)
        rtx[8 * k : 8 * k + 8] = packed.reshape(8, 16, 512)
        for place in range(8 * k, 8 * k + 8):
            if place == 0:
                rrx[0] = packed[0:16]
                continue
            copy = pltpu.make_async_remote_copy(
                src_ref=rtx.at[place], dst_ref=rrx.at[place], send_sem=tsem.at[32 + place],
                recv_sem=rsem.at[32 + place], device_id=source(place), device_id_type=MESH,
            )
            copy.start()
            returned.append(copy)

    proj = {}

    def project():
        arrive("xa", "wq", "wk", "wv", "dd", "rd", "shift", "spike")
        normed = rms(v_xa[...], gain_a[...])
        qkv = dot(normed, v_qkv[...])
        last = ((1,), (1,))
        low = jnp.tanh(dot(normed, v_dd[...], last)).astype(BF)
        logits = decay_bias[...] + dot(low, decay_up[...]) + v_shift[...]
        log_decay = v_spike[...] - ROOT * sigmoid(logits)
        rate_low = dot(normed, v_rd[...], last).astype(BF)
        rate = sigmoid(rate_base[...] + dot(rate_low, rate_up[...]))
        q, k, v = qkv[:, 0:256], qkv[:, 256:512], qkv[:, 512:768]
        same = ones_where((iota((256, 256), 0) >> 6) == (iota((256, 256), 1) >> 6))
        unit = k * lax.rsqrt(dot_exact_right(k * k, same) + unit_eps)
        write = unit * rate
        block = (row >> 5) == (lane >> 5)
        cum = dot_exact_left(ones_where(block & (lane <= row)), log_decay)
        total = dot_exact_left(ones_where(block), log_decay)
        middle = 0.5 * total
        fade_in = jnp.exp(cum - middle)
        fade_out = jnp.exp(middle - cum)
        proj["qf"] = q * fade_in
        proj["ef"] = -unit * jnp.exp(cum - log_decay - middle)
        proj["wf"] = write * fade_out
        proj["kf"] = k * fade_out
        proj["v"] = v
        proj["em"] = jnp.exp(middle)
        proj["end"] = jnp.exp(total)

    def head(h):
        at = slice(HEAD * h, HEAD * h + HEAD)
        qf, ef, wf, kf, v, em, end = (proj[n][:, at] for n in ("qf", "ef", "wf", "kf", "v", "em", "end"))
        last = ((1,), (1,))
        block = (row >> 5) == (lane >> 5)
        strict, upto = block & (lane < row), block & (lane <= row)
        erase_write = jnp.where(strict, dot(ef, wf, last), 0.0)
        erase_key = jnp.where(strict, dot(ef, kf, last), 0.0)
        query_write = jnp.where(upto, dot(qf, wf, last), 0.0)
        query_key = jnp.where(upto, dot(qf, kf, last), 0.0)
        inverse = jnp.where(row == lane, 1.0, 0.0)
        for level in range(5):
            size = 1 << level
            corner = ((row >> (level + 1)) == (lane >> (level + 1))) & ((row & size) != 0) & ((lane & size) == 0)
            off = jnp.where(corner, erase_write, 0.0)
            if level == 0:
                inverse = inverse + off
            else:
                inverse = inverse + dot3(dot3(inverse, off), inverse)
        right = jnp.concatenate([ef * em, dot(erase_key, v)], axis=1)
        held = dot3(inverse, right)
        shown = dot(query_write, held) + jnp.concatenate([qf * em, dot(query_key, v)], axis=1)
        wide = (128, 256)
        mine_only = (iota(wide, 0) >> 5) == (iota(wide, 1) >> 6)
        ends_w = jnp.where(mine_only, jnp.concatenate([wf * em] * 4, axis=1), 0.0)
        ends_k = jnp.where(mine_only, jnp.concatenate([kf * em] * 4, axis=1), 0.0)
        ends = jnp.concatenate([ends_w, ends_k], axis=0)
        felt = jnp.concatenate([held, jnp.concatenate([jnp.zeros_like(v), v], axis=1)], axis=0)
        maps = dot(ends.T, felt)
        lane2, row2 = iota((HEAD, 128), 1), iota((HEAD, 128), 0)
        state = jnp.where(lane2 == row2, 1.0, 0.0)
        pieces = []
        for n in range(4):
            t = slice(SPAN * n, SPAN * n + SPAN)
            piece = dot3(shown[t, 0:HEAD], state)
            pieces.append(piece + jnp.where(iota((SPAN, 128), 1) >= HEAD, shown[t], 0.0))
            fade = jnp.concatenate([end[SPAN * n : SPAN * n + 1]] * 2, axis=1)
            step = maps[HEAD * n : HEAD * n + HEAD] + jnp.where(lane2 == row2, fade, 0.0)
            state = step if n == 0 else compose(step, state)
        umat[h] = jnp.concatenate(pieces, axis=0)
        atx[h] = state.astype(BF)

    scan = {}

    def scan1():
        arx[0] = atx[x]
        scan["x"] = [
            send(atx.at[(x + d) & 3], arx.at[d], {"x": (x + d) & 3}) for d in range(1, 4)
        ]

    def scan2():
        for copy in scan["x"]:
            copy.wait_recv()
        state = arx[x & 3].astype(F32)
        cmat[0] = state
        for n in range(1, 4):
            state = compose(arx[(x - n) & 3].astype(F32), state)
            cmat[n] = state
        ztx[...] = state.astype(BF)
        zrx[0] = ztx[...]
        scan["z"] = [send(ztx, zrx.at[d], {"z": (z + d) & 7}) for d in range(1, 8)]

    def scan3():
        for copy in scan["z"]:
            copy.wait_recv()
        lane2, row2 = iota((HEAD, 128), 1), iota((HEAD, 128), 0)
        state = jnp.where(lane2 == row2, 1.0, 0.0)
        for n in range(7):
            after = compose(zrx[(z - n) & 7].astype(F32), state)
            state = jnp.where(jnp.broadcast_to(n < z, after.shape), after, state)
        btx[0] = state.astype(BF)
        for n in range(1, 4):
            btx[n] = compose(cmat[n - 1], state).astype(BF)
        brx[0] = btx[x]
        scan["b"] = [
            send(btx.at[(x + d) & 3], brx.at[d], {"x": (x + d) & 3}) for d in range(1, 4)
        ]

    def finish_heads():
        for copy in scan["b"]:
            copy.wait_recv()
        outs = []
        for h in range(4):
            u = umat[h]
            outs.append((u + dot3(u[:, 0:HEAD], brx[(x - h) & 3].astype(F32)))[:, HEAD:])
        out = jnp.concatenate(outs, axis=1)
        same = ones_where((iota((256, 256), 0) >> 6) == (iota((256, 256), 1) >> 6))
        centered = out - dot_exact_right(out, same) * (1.0 / HEAD)
        var = dot_exact_right(centered * centered, same) * (1.0 / HEAD)
        mixed[...] = (centered * lax.rsqrt(var + group_eps) * head_gain[...].astype(F32)).astype(BF)

    def project_out():
        arrive("out")
        rows = jnp.concatenate(
            [
                mixed[pl.ds(pl.multiple_of(16 * (2 * ((y + r) & 3) + side), 16), 16), :]
                for side in (c, cc)
                for r in range(4)
            ],
            axis=0,
        )
        YA[...] = dot(rows, v_out[...]).astype(BF).reshape(2, 4, 16, 2048)

    project()
    gather2(4)
    unpack(0)
    gather1(0)
    head(0)
    gather3(4)
    unpack(1)
    gather1(1)
    head(1)
    gather2(0)
    unpack(2)
    gather1(2)
    gather4(4)
    arrive("sg", "su", "sd")
    shared_expert()
    sum1(4)
    head(2)
    gather3(0)
    gather2(1)
    unpack(3)
    gather1(3)
    sum2(4)
    head(3)
    scan1()
    gather2(2)
    gather3(1)
    gather4(0)
    arrive("eg", "eu", "ed")
    experts(0)
    sum1(0)
    sum3(4)
    scan2()
    gather2(3)
    gather3(2)
    gather4(1)
    experts(1)
    sum1(1)
    sum2(0)
    scan3()
    gather3(3)
    gather4(2)
    experts(2)
    sum1(2)
    sum2(1)
    sum3(0)
    finish_heads()
    gather4(3)
    experts(3)
    sum1(3)
    sum2(2)
    sum3(1)
    project_out()
    sum1("a")
    give_back(0)
    sum2(3)
    sum3(2)
    sum2("a")
    give_back(1)
    sum3(3)
    give_back(2)
    sum3("a")
    give_back(3)
    out_a[...] = sum4("a").astype(BF)
    total = sum4(4)
    routed = None
    for k in range(4):
        for place in range(8 * k, 8 * k + 8):
            if place:
                returned[place - 1].wait_recv()
        tiles = rrx[8 * k : 8 * k + 8].reshape(128, 512)
        at = slice(128 * k, 128 * k + 128)
        part = dot(sel_hi[at].T, tiles) + dot(sel_lo[at].T, tiles)
        routed = part if routed is None else routed + part
    out_b[...] = (quarter_lanes(routed, 32) + total).astype(BF)
    for copy in started + dispatched + returned:
        copy.wait_send()


SENDS = 110


def per_device(
    xa, gain_a, wq, wk, wv, decay_down, decay_up, decay_bias, decay_shift, decay_spike,
    rate_down, rate_up, rate_base, head_gain, w_out, xb, gain_b, ids, weights,
    e_gate, e_up, e_down, s_gate, s_up, s_down,
):
    here = pl.BlockSpec(memory_space=pltpu.VMEM)
    away = pl.BlockSpec(memory_space=pl.ANY)
    operands = [
        (xa, away), (gain_a[None], here), (wq, away), (wk, away), (wv, away),
        (decay_down.T, away), (decay_up, here), (decay_bias[None], here),
        (decay_shift, away), (decay_spike, away), (rate_down.T, away), (rate_up, here),
        (rate_base[None], here), (head_gain[None], here), (w_out, away), (xb, here),
        (gain_b[None], here), (ids.T, here), (weights.T, here), (e_gate, away), (e_up, away),
        (e_down, away), (s_gate, away), (s_up, away), (s_down, away),
    ]
    vm = pltpu.VMEM
    sums = lambda n: [
        vm((4, n, 2048), BF), vm((4, n, 2048), BF)] + [vm((n, HALF), BF)] * 8
    stacked = [vm((5,) + s.shape, BF) for s in sums(32)]
    scratch = [
        vm((128, 2048), BF), vm((2048, 768), BF), vm((64, 2048), BF), vm((64, 2048), BF),
        vm((128, 256), F32), vm((128, 256), F32), vm((256, 2048), BF), vm((2, 2048, 256), BF),
        vm((2, 128, 2048), BF), vm((2048, 256), BF), vm((128, 2048), BF),
        vm((32, 16, 512), BF), vm((32, 16, 512), BF), vm((32, 16, 512), BF), vm((32, 16, 512), BF),
        vm((5, 2, 4, 32, 2048), BF), vm((5, 2, 4, 32, 2048), BF),
        *stacked,
        vm((2, 4, 16, 2048), BF), *sums(16),
        vm((4, 64, 128), F32), vm((4, 128, 128), F32), vm((128, 256), BF),
        vm((4, 64, 128), BF), vm((4, 64, 128), BF), vm((64, 128), BF), vm((8, 64, 128), BF),
        vm((4, 64, 128), BF), vm((4, 64, 128), BF), vm((512, 128), BF), vm((512, 128), BF),
        pltpu.SemaphoreType.DMA((15,)), pltpu.SemaphoreType.DMA((64,)), pltpu.SemaphoreType.DMA((64,)),
        pltpu.SemaphoreType.DMA((SENDS,)), pltpu.SemaphoreType.DMA((SENDS,)),
    ]
    return pl.pallas_call(
        kernel,
        out_shape=(jax.ShapeDtypeStruct((16, 2048), BF), jax.ShapeDtypeStruct((32, 2048), BF)),
        in_specs=[spec for _, spec in operands],
        out_specs=(here, here),
        scratch_shapes=scratch,
        compiler_params=pltpu.CompilerParams(
            collective_id=0, has_side_effects=True, vmem_limit_bytes=60 * 1024 * 1024
        ),
    )(*[array for array, _ in operands])


def solution(mesh):
    split_mesh = Mesh(mesh.devices.reshape(8, 4, 4, 2), ("z", "x", "y", "c"))
    ep, tp = ("z", "x"), ("y", "c")
    both = ep + tp
    return jax.shard_map(
        per_device,
        mesh=split_mesh,
        in_specs=(
            P(ep, None), P(), P(None, tp), P(None, tp), P(None, tp), P(), P(None, tp), P(tp),
            P(ep, tp), P(ep, tp), P(), P(None, tp), P(tp), P(tp), P(tp, None), P(both, None),
            P(), P(ep, None), P(both, None), P(ep, None, tp), P(ep, None, tp), P(ep, tp, None),
            P(None, tp), P(None, tp), P(tp, None),
        ),
        out_specs=(P(both, None), P(both, None)),
        check_vma=False,
    )
```

time: 307 us -> 87.9 us (0.29); the launches traced: 303 us -> 87.7 us
  Pallas kernels: 0 us -> 82.4 us
  matrix products: 70.6 us -> 0 us
  blocking collectives: 61.3 us -> 0 us
  other arithmetic: 51.3 us -> 0 us
  starting transfers between devices: 45.9 us -> 0 us
  local copies, waits for them, and re-layouts: 35.8 us -> 4.7 us
  waiting for transfers between devices: 22.5 us -> 0 us
  between operations: 15 us -> 0.67 us
    pallas_call x0 -> x1, Pallas kernels: none -> 82.4 us  [per_device(): pl.pallas_call(kernel, out_shape=(jax.ShapeDtypeStruct((16, 2048), BF), j...]
    dot_general x89 -> x0, matrix products: 69.3 us -> none  [the longest x1 8.61 us: per_device(): jnp.einsum('tgjcf,jfd->tgjcd', hidden, expert_down_weight, preferred_elem...]
    all_gather x4 -> x0, blocking collectives: 61.3 us -> none  [prefix_by_axis(): lax.all_gather(part.astype(kind), axis)]
    all_to_all x4 -> x0, starting transfers between devices: 45.9 us -> none  [the longest x1 20.8 us: summed_on_arrival(): lax.all_to_all(blocks, axis, split_axis=0, concat_axis=0, tiled=True)]
    another operation x30 -> x0, other arithmetic: 40.2 us -> none  [the longest x20 39.8 us: block_tables(): jax.scipy.linalg.solve_triangular(identity - erase_write, identity, lower...]
    all_to_all x4 -> x0, waiting for transfers between devices: 21.7 us -> none  [the longest x1 14.4 us: per_device(): lax.all_to_all(expert_out, EP, split_axis=0, concat_axis=0, tiled=True)]
    concatenate x3 -> x0, local copies, waits for them, and re-layouts: 5.51 us -> none  [the longest x1 5.41 us: per_device(): jnp.concatenate([routed_part.reshape(block_total, routed_rows, model_widt...]
    dynamic_update_slice x12 -> x0, local copies, waits for them, and re-layouts: 5.21 us -> none  [per_device(): lax.map(lambda block_items: block_tables(*block_items), (to_blocks(query_...]
  transfers between devices with their start and end apart: 6 -> 0, of which waited for: 2 -> 0; matrix products, arithmetic and copies ran while one was open for 38% -> 0% of each run, Pallas kernels for 0% -> 0%
where the time goes in v1:
time: 87.9 us; the launch traced here: 87.7 us
  Pallas kernels  82.4 us (94%)
  local copies, waits for them, and re-layouts  4.7 us (5%)
    pallas_call x1, Pallas kernels, per_device(): pl.pallas_call(kernel, out_shape=(jax.ShapeDtypeStruct((16, 2048), BF), j...  82.4 us
    unnamed x10, local copies, waits for them, and re-layouts  2.91 us

profile of v1, /device:TPU:1, one launch (start us, length us, event | category | flops | bytes accessed | tf_op | source)
XLA Modules:
  0.0 87.7 jit_solution(4161544841639356821)
XLA Ops:
  0.6 0.0 copy-start.1
  0.6 0.0 copy-start.3
  0.6 0.7 copy-done.3
  1.3 0.6 broadcast_in_dim.18.head_gain
  1.9 0.0 copy-done.1
  1.9 0.0 copy-start.2
  1.9 0.6 broadcast_in_dim.15.gain_a
  2.5 0.1 copy-done.2
  2.6 0.6 broadcast_in_dim.19.gain_b
  3.2 82.4 %shard_map.248 = (bf16[16,2048]{1,0:T(8,128)(2,1)}, bf16[32,2048]{1,0:T(8,128)(2,1)}) custom-call(bf16[128,2048]{1,0:T(8,128)(2,1)} %xa.1, bf16[1,2048]{1,0:T(2,128)(2,1)} %broadcast_in_dim.15.gain_a, bf16[2048,256]{1,0:T(8,128)(2,1)} %wq.1, bf16[2048,256]{1,0:T(8,128)(2,1)} %wk.1, bf16[2048,256]{1,0:T(8,128)(2,1)} %wv.1, bf16[64,2048]{1,0:T(8,128)(2,1)} %bitcast.6, ...), custom_call_target="tpu_custom_call" | custom-call | tf_op jit(solution)/shard_map/pallas_call | solution.py:565
  85.6 0.0 copy-start
  85.6 1.5 %copy.29 = bf16[16,2048]{1,0:T(8,128)(2,1)} copy(bf16[16,2048]{1,0:T(8,128)(2,1)} %get-tuple-element.4) | data formatting | bytes 131072
  87.1 0.0 copy-done
  87.1 0.7 copy.30
Async XLA Ops:
  0.6 1.3 %copy-start.1 = (bf16[2048]{0:T(1024)(128)(2,1)S(1)}, bf16[2048]{0:T(1024)(128)(2,1)}, u32[]{:S(2)}) copy-start(bf16[2048]{0:T(1024)(128)(2,1)} %param.26) | copy-start | bytes 12292
  0.6 0.7 copy-start.3
  1.9 0.7 copy-start.2
  85.6 1.5 %copy-start = (bf16[32,2048]{1,0:T(8,128)(2,1)S(1)}, bf16[32,2048]{1,0:T(8,128)(2,1)}, u32[]{:S(2)}) copy-start(bf16[32,2048]{1,0:T(8,128)(2,1)} %get-tuple-element.5) | copy-start | bytes 393220

commit v2 on v1

v2 whole, which is shorter than its diff:
```python
import jax
import jax.numpy as jnp
from jax import lax
from jax.experimental import pallas as pl
from jax.experimental.pallas import tpu as pltpu
from jax.sharding import Mesh
from jax.sharding import PartitionSpec as P

MESH = pl.DeviceIdType.MESH
BF, F32 = jnp.bfloat16, jnp.float32
norm_eps = 1e-06
group_eps = 0.00064
unit_eps = 1e-06
ROOT = 0.6065306597126334

HEADS = 4
HEAD = 64
SPAN = 32
ROWS = 128
TOK = 32
CHUNKS = 4
HALF = 1024
DZ = (7, 2, 6, 3, 5, 4, 0, 1)
OWN = 24
PLACES = [place for place in range(32) if place != OWN]
TABLE = sum(d << (3 * n) for n, d in enumerate(DZ))


def iota(shape, dim):
    return lax.broadcasted_iota(jnp.int32, shape, dim)


def dot(a, b, dims=((1,), (0,))):
    return lax.dot_general(a.astype(BF), b.astype(BF), (dims, ((), ())), preferred_element_type=F32)


def split(a):
    high = a.astype(BF)
    return high, (a - high.astype(F32)).astype(BF)


def dot3(a, b):
    ah, al = split(a)
    bh, bl = split(b)
    return dot(ah, bh) + (dot(ah, bl) + dot(al, bh))


def dot_exact_left(a, b):
    bh, rest = b.astype(BF), None
    rest = b - bh.astype(F32)
    bm = rest.astype(BF)
    bl = (rest - bm.astype(F32)).astype(BF)
    return dot(a, bh) + (dot(a, bm) + dot(a, bl))


def dot_exact_right(a, b):
    ah = a.astype(BF)
    rest = a - ah.astype(F32)
    am = rest.astype(BF)
    al = (rest - am.astype(F32)).astype(BF)
    return dot(ah, b) + (dot(am, b) + dot(al, b))


def sigmoid(u):
    e = jnp.exp(-jnp.abs(u))
    return jnp.where(u >= 0, 1.0, e) / (1.0 + e)


def rms(values, gain):
    values = values.astype(F32)
    scaled = values * lax.rsqrt(jnp.mean(values * values, axis=-1, keepdims=True) + norm_eps)
    return (scaled * gain.astype(F32)).astype(BF)


def ones_where(mask, kind=BF):
    return jnp.where(mask, 1.0, 0.0).astype(kind)


def row_of(ref):
    return ref[...].reshape(1, ref.shape[0])


def compose(later, earlier):
    lane = iota(later.shape, 1)
    return dot3(later[:, :HEAD], earlier) + jnp.where(lane >= HEAD, later, 0.0)


def quarter_rows(matrix):
    return jnp.concatenate([matrix[:, 512 * q : 512 * (q + 1)] for q in range(4)], axis=0)


def quarter_lanes(matrix, rows):
    return jnp.concatenate([matrix[rows * q : rows * (q + 1)] for q in range(4)], axis=1)


def kernel(
    xa, h_gain_a, wq, wk, wv, decay_down, h_decay_up, h_decay_bias, decay_shift, decay_spike,
    rate_down, h_rate_up, h_rate_base, h_head_gain, w_out, h_xb, h_gain_b, h_ids, h_weights,
    e_gate, e_up, e_down, s_gate, s_up, s_down,
    out_a, out_b,
    v_xa, v_qkv, v_dd, v_rd, v_shift, v_spike, v_out, v_egu, v_ed, v_sgu, v_sd,
    gain_a, decay_up, decay_bias, rate_up, rate_base, head_gain, xb, gain_b, ids, weights,
    tx, rx, rtx, rrx, X, Y, PR, Z, RA, RB, FA, FD, FB, FE, CA, CB,
    YA, PA, ZA, RAa, RBa, FAa, FDa, FBa, FEa, CAa, CBa,
    cmat, umat, mixed, atx, arx, ztx, zrx, btx, brx, sel_hi, sel_lo,
    lsem, ssend, srecv,
):
    z, x, y, c = (lax.axis_index(name) for name in ("z", "x", "y", "c"))
    yp, ym, cc = (y + 1) & 3, (y + 3) & 3, 1 - c

    barrier = pltpu.get_barrier_semaphore()

    def peer(place):
        return {"z": (z + DZ[place // 4]) & 7, "x": (x + place % 4) & 3}

    def source(place):
        return {"z": (z - DZ[place // 4]) & 7, "x": (x - place % 4) & 3}

    for place in PLACES:
        pl.semaphore_signal(barrier, inc=1, device_id=peer(place), device_id_type=MESH)
    for target in ({"y": yp}, {"y": ym}, {"c": cc}):
        pl.semaphore_signal(barrier, inc=1, device_id=target, device_id_type=MESH)

    local = {}

    def fetch(name, src, dst):
        copy = pltpu.make_async_copy(src, dst, lsem.at[len(local)])
        copy.start()
        local[name] = copy

    fetch("xb", h_xb, xb)
    fetch("gain_b", h_gain_b, gain_b)
    fetch("ids", h_ids, ids)
    fetch("weights", h_weights, weights)
    fetch("xa", xa, v_xa)
    fetch("gain_a", h_gain_a, gain_a)
    fetch("decay_up", h_decay_up, decay_up)
    fetch("decay_bias", h_decay_bias, decay_bias)
    fetch("rate_up", h_rate_up, rate_up)
    fetch("rate_base", h_rate_base, rate_base)
    fetch("head_gain", h_head_gain, head_gain)
    fetch("wq", wq, v_qkv.at[:, 0:256])
    fetch("wk", wk, v_qkv.at[:, 256:512])
    fetch("wv", wv, v_qkv.at[:, 512:768])
    fetch("dd", decay_down, v_dd)
    fetch("rd", rate_down, v_rd)
    fetch("shift", decay_shift, v_shift)
    fetch("spike", decay_spike, v_spike)
    fetch("sg", s_gate, v_sgu.at[:, 0:128])
    fetch("su", s_up, v_sgu.at[:, 128:256])
    fetch("sd", s_down, v_sd)
    fetch("eg", e_gate, v_egu.at[:, :, 0:128])
    fetch("eu", e_up, v_egu.at[:, :, 128:256])
    fetch("ed", e_down, v_ed)
    fetch("out", w_out, v_out)

    def arrive(*names):
        for name in names:
            local[name].wait()

    send_names, recv_names = {}, {}

    def send(src, dst, target, leaving, landing):
        pltpu.make_async_remote_copy(
            src_ref=src, dst_ref=dst,
            send_sem=ssend.at[send_names.setdefault(leaving, len(send_names))],
            recv_sem=srecv.at[recv_names.setdefault(landing, len(recv_names))],
            device_id=target, device_id_type=MESH,
        ).start()

    def take(ref, landing):
        pltpu.make_async_copy(ref, ref, srecv.at[recv_names[landing]]).wait()

    def sent(ref, leaving):
        pltpu.make_async_copy(ref, ref, ssend.at[send_names[leaving]]).wait()

    arrive("xb", "gain_b", "ids", "weights")
    normed_b = rms(xb[...], row_of(gain_b))
    mine = 32 * (2 * y + c)
    pick = ones_where(iota((256, 128), 0) == mine + (iota((256, 128), 1) & 31))
    own_ids = dot(ids[...].astype(F32), pick).astype(jnp.int32)
    expert = iota((128, 128), 0) >> 1
    first, second = own_ids[0:1] == expert, own_ids[1:2] == expert
    named = ones_where(first | second)
    lane, row = iota((128, 128), 1), iota((128, 128), 0)
    earlier = ones_where(((row >> 5) == (lane >> 5)) & (row < lane))
    count = dot(named, earlier)
    taken = (first | second) & (count == (row & 1).astype(F32))
    spread = ones_where((iota((32, 128), 1) & 31) == iota((32, 128), 0))
    w_tiled = dot_exact_right(weights[...], spread)
    slot_weight = jnp.where(taken, jnp.where(first, w_tiled[0:1], w_tiled[1:2]), 0.0)
    R, S = iota((512, 128), 0), iota((512, 128), 1)
    dz = lax.shift_right_logical(jnp.full_like(R, TABLE), 3 * (R >> 6)) & 7
    group = (((z + dz) & 7) << 2) + ((x + ((R >> 4) & 3)) & 3)
    place_of = ones_where(S == (group << 2) + (R & 3))
    own_quarter = ((R >> 2) & 3) == (S >> 5)
    chosen = jnp.where(own_quarter, dot(place_of, ones_where(taken)), 0.0)
    outgoing = dot(chosen, quarter_rows(normed_b)).astype(BF)
    tx[...] = outgoing.reshape(32, 16, 512)
    rx[OWN] = outgoing[16 * OWN : 16 * OWN + 16]
    X[4, 0] = normed_b

    pl.semaphore_wait(barrier, 34)
    for place in PLACES:
        send(tx.at[place], rx.at[place], peer(place), "d", ("d", place // 8))

    def tiles_of(ref, k):
        return ref.at[OWN + 1 : 32] if k == OWN // 8 else ref.at[8 * k : 8 * k + 8]

    def gather1(k):
        own = X.at[k, 0]
        send(own, X.at[k, 3], {"y": yp}, ("g", k), ("gl", k))
        send(own, X.at[k, 1], {"y": ym}, ("g", k), ("gr", k))
        send(own, X.at[k, 4], {"c": cc}, ("g", k), ("gc", k))

    def gather2(k):
        left, right = X.at[k, 3], X.at[k, 1]
        take(left, ("gl", k))
        send(left.at[:, 0:HALF], X.at[k, 2, :, 0:HALF], {"y": yp}, ("g", k), ("gh", k))
        send(left, X.at[k, 7], {"c": cc}, ("g", k), ("gc", k))
        take(right, ("gr", k))
        send(right.at[:, HALF:], X.at[k, 2, :, HALF:], {"y": ym}, ("g", k), ("gh", k))
        send(right, X.at[k, 5], {"c": cc}, ("g", k), ("gc", k))

    def gather3(k):
        take(X.at[k, 2], ("gh", k))
        send(X.at[k, 2], X.at[k, 6], {"c": cc}, ("g", k), ("gc", k))

    def gather4(k):
        take(X.at[k, 4:8], ("gc", k))

    gather1(4)

    by_place = [jnp.where(own_quarter, dot(place_of, part), 0.0).astype(BF) for part in split(slot_weight)]
    sel_hi[...], sel_lo[...] = by_place

    def tile_row(a):
        return (((a >> 1) & 7) << 4) + ((a >> 5) << 2) + (((a >> 4) & 1) << 1) + (a & 1)

    def unpack_matrix():
        return ones_where(lane == tile_row(row))

    def pack_matrix():
        return ones_where(row == tile_row(lane))

    def unpack(k):
        take(tiles_of(rx, k), ("d", k))
        tiles = rx[8 * k : 8 * k + 8].reshape(128, 512)
        stacked = dot(unpack_matrix(), tiles).astype(BF)
        X[k, 0] = quarter_lanes(stacked, 32)

    def hidden_of(rows, gate_up):
        both = dot(rows, gate_up)
        gate = both[:, 0:128]
        return (gate * sigmoid(gate) * both[:, 128:256]).astype(BF)

    def experts(k):
        for j in range(2):
            rows = X[k, :, 16 * j : 16 * j + 16, :].reshape(128, 2048)
            hidden = hidden_of(rows, v_egu[j])
            Y[k, :, 16 * j : 16 * j + 16, :] = dot(hidden, v_ed[j]).astype(BF).reshape(8, 16, 2048)

    def shared_expert():
        rows = X[4].reshape(256, 2048)
        hidden = hidden_of(rows, v_sgu[...])
        Y[4] = dot(hidden, v_sd[...]).astype(BF).reshape(8, 32, 2048)

    def refs_of(k):
        if k == "a":
            return YA, PA, ZA, RAa, RBa, FAa, FDa, FBa, FEa, CAa, CBa
        return tuple(ref.at[k] for ref in (Y, PR, Z, RA, RB, FA, FD, FB, FE, CA, CB))

    def sum1(k):
        refs = refs_of(k)
        send(refs[0].at[4:8], refs[1], {"c": cc}, ("s", k), ("sp", k))

    def sum2(k):
        part, pair, total, ra, rb, fa, fd, fb, fe, ca, cb = refs_of(k)
        take(pair, ("sp", k))
        total[...] = (part[0:4].astype(F32) + pair[...].astype(F32)).astype(BF)
        send(total.at[2, :, 0:HALF], ra, {"y": yp}, ("s", k), ("sa", k))
        send(total.at[2, :, HALF:], rb, {"y": ym}, ("s", k), ("sb", k))
        send(total.at[1, :, HALF:], fe, {"y": yp}, ("s", k), ("sf", k))
        send(total.at[3, :, 0:HALF], fd, {"y": ym}, ("s", k), ("sf", k))

    def sum3(k):
        part, pair, total, ra, rb, fa, fd, fb, fe, ca, cb = refs_of(k)
        take(ra, ("sa", k))
        ca[...] = (total[1, :, 0:HALF].astype(F32) + ra[...].astype(F32)).astype(BF)
        send(ca, fa, {"y": yp}, ("s", k), ("sf", k))
        take(rb, ("sb", k))
        cb[...] = (total[3, :, HALF:].astype(F32) + rb[...].astype(F32)).astype(BF)
        send(cb, fb, {"y": ym}, ("s", k), ("sf", k))

    def sum4(k):
        part, pair, total, ra, rb, fa, fd, fb, fe, ca, cb = refs_of(k)
        take(total.at[0:2], ("sf", k))
        low = total[0, :, 0:HALF].astype(F32) + (fa[...].astype(F32) + fd[...].astype(F32))
        high = total[0, :, HALF:].astype(F32) + (fb[...].astype(F32) + fe[...].astype(F32))
        return jnp.concatenate([low, high], axis=1)

    def give_back(k):
        stacked = quarter_rows(sum4(k).astype(BF))
        packed = dot(pack_matrix(), stacked).astype(BF)
        rtx[8 * k : 8 * k + 8] = packed.reshape(8, 16, 512)
        for place in range(8 * k, 8 * k + 8):
            if place == OWN:
                rrx[OWN] = packed[0:16]
            else:
                send(rtx.at[place], rrx.at[place], source(place), "r", ("r", k))

    proj = {}

    def project():
        arrive("xa", "gain_a", "wq", "wk", "wv", "dd", "rd", "shift", "spike")
        arrive("decay_up", "decay_bias", "rate_up", "rate_base", "head_gain")
        normed = rms(v_xa[...], row_of(gain_a))
        qkv = dot(normed, v_qkv[...])
        last = ((1,), (1,))
        low = jnp.tanh(dot(normed, v_dd[...], last)).astype(BF)
        logits = decay_bias[...] + dot(low, decay_up[...]) + v_shift[...]
        log_decay = v_spike[...] - ROOT * sigmoid(logits)
        rate_low = dot(normed, v_rd[...], last).astype(BF)
        rate = sigmoid(rate_base[...] + dot(rate_low, rate_up[...]))
        q, k, v = qkv[:, 0:256], qkv[:, 256:512], qkv[:, 512:768]
        same = ones_where((iota((256, 256), 0) >> 6) == (iota((256, 256), 1) >> 6))
        unit = k * lax.rsqrt(dot_exact_right(k * k, same) + unit_eps)
        write = unit * rate
        block = (row >> 5) == (lane >> 5)
        cum = dot_exact_left(ones_where(block & (lane <= row)), log_decay)
        total = dot_exact_left(ones_where(block), log_decay)
        middle = 0.5 * total
        fade_in = jnp.exp(cum - middle)
        fade_out = jnp.exp(middle - cum)
        proj["qf"] = q * fade_in
        proj["ef"] = -unit * jnp.exp(cum - log_decay - middle)
        proj["wf"] = write * fade_out
        proj["kf"] = k * fade_out
        proj["v"] = v
        proj["em"] = jnp.exp(middle)
        proj["end"] = jnp.exp(total)

    def head(h):
        at = slice(HEAD * h, HEAD * h + HEAD)
        qf, ef, wf, kf, v, em, end = (proj[n][:, at] for n in ("qf", "ef", "wf", "kf", "v", "em", "end"))
        last = ((1,), (1,))
        block = (row >> 5) == (lane >> 5)
        strict, upto = block & (lane < row), block & (lane <= row)
        erase_write = jnp.where(strict, dot(ef, wf, last), 0.0)
        erase_key = jnp.where(strict, dot(ef, kf, last), 0.0)
        query_write = jnp.where(upto, dot(qf, wf, last), 0.0)
        query_key = jnp.where(upto, dot(qf, kf, last), 0.0)
        yield
        inverse = jnp.where(row == lane, 1.0, 0.0)
        for level in range(5):
            size = 1 << level
            corner = ((row >> (level + 1)) == (lane >> (level + 1))) & ((row & size) != 0) & ((lane & size) == 0)
            off = jnp.where(corner, erase_write, 0.0)
            if level == 0:
                inverse = inverse + off
            else:
                inverse = inverse + dot3(dot3(inverse, off), inverse)
                yield
        right = jnp.concatenate([ef * em, dot(erase_key, v)], axis=1)
        held = dot3(inverse, right)
        shown = dot(query_write, held) + jnp.concatenate([qf * em, dot(query_key, v)], axis=1)
        yield
        wide = (128, 256)
        mine_only = (iota(wide, 0) >> 5) == (iota(wide, 1) >> 6)
        ends_w = jnp.where(mine_only, jnp.concatenate([wf * em] * 4, axis=1), 0.0)
        ends_k = jnp.where(mine_only, jnp.concatenate([kf * em] * 4, axis=1), 0.0)
        ends = jnp.concatenate([ends_w, ends_k], axis=0)
        felt = jnp.concatenate([held, jnp.concatenate([jnp.zeros_like(v), v], axis=1)], axis=0)
        maps = dot(ends.T, felt)
        yield
        lane2, row2 = iota((HEAD, 128), 1), iota((HEAD, 128), 0)
        state = jnp.where(lane2 == row2, 1.0, 0.0)
        pieces = []
        for n in range(4):
            t = slice(SPAN * n, SPAN * n + SPAN)
            piece = dot3(shown[t, 0:HEAD], state)
            pieces.append(piece + jnp.where(iota((SPAN, 128), 1) >= HEAD, shown[t], 0.0))
            fade = jnp.concatenate([end[SPAN * n : SPAN * n + 1]] * 2, axis=1)
            step = maps[HEAD * n : HEAD * n + HEAD] + jnp.where(lane2 == row2, fade, 0.0)
            state = step if n == 0 else compose(step, state)
            yield
        umat[h] = jnp.concatenate(pieces, axis=0)
        atx[h] = state.astype(BF)
        yield

    walks = []

    def heads(steps):
        if not walks:
            walks.extend(head(h) for h in range(HEADS))
        for _ in range(steps):
            for walk in walks:
                next(walk)

    def scan1():
        arx[0] = atx[x]
        for d in range(1, 4):
            send(atx.at[(x + d) & 3], arx.at[d], {"x": (x + d) & 3}, "x", "x")

    def scan2():
        take(arx.at[1:4], "x")
        state = arx[x & 3].astype(F32)
        cmat[0] = state
        for n in range(1, 4):
            state = compose(arx[(x - n) & 3].astype(F32), state)
            cmat[n] = state
        ztx[...] = state.astype(BF)
        zrx[0] = ztx[...]
        for d in range(1, 8):
            send(ztx, zrx.at[d], {"z": (z + d) & 7}, "z", "z")

    def scan3():
        take(zrx.at[1:8], "z")
        lane2, row2 = iota((HEAD, 128), 1), iota((HEAD, 128), 0)
        state = jnp.where(lane2 == row2, 1.0, 0.0)
        for n in range(7):
            after = compose(zrx[(z - n) & 7].astype(F32), state)
            state = jnp.where(jnp.broadcast_to(n < z, after.shape), after, state)
        btx[0] = state.astype(BF)
        for n in range(1, 4):
            btx[n] = compose(cmat[n - 1], state).astype(BF)
        brx[0] = btx[x]
        for d in range(1, 4):
            send(btx.at[(x + d) & 3], brx.at[d], {"x": (x + d) & 3}, "b", "b")

    def finish_heads():
        take(brx.at[1:4], "b")
        outs = []
        for h in range(4):
            u = umat[h]
            outs.append((u + dot3(u[:, 0:HEAD], brx[(x - h) & 3].astype(F32)))[:, HEAD:])
        out = jnp.concatenate(outs, axis=1)
        same = ones_where((iota((256, 256), 0) >> 6) == (iota((256, 256), 1) >> 6))
        centered = out - dot_exact_right(out, same) * (1.0 / HEAD)
        var = dot_exact_right(centered * centered, same) * (1.0 / HEAD)
        mixed[...] = (centered * lax.rsqrt(var + group_eps) * row_of(head_gain).astype(F32)).astype(BF)

    def project_out():
        arrive("out")
        rows = jnp.concatenate(
            [
                mixed[pl.ds(pl.multiple_of(16 * (2 * ((y + r) & 3) + side), 16), 16), :]
                for side in (c, cc)
                for r in range(4)
            ],
            axis=0,
        )
        YA[...] = dot(rows, v_out[...]).astype(BF).reshape(8, 16, 2048)

    project()
    heads(2)
    gather2(4)
    unpack(0)
    gather1(0)
    heads(2)
    unpack(1)
    gather1(1)
    heads(1)
    gather2(0)
    heads(1)
    unpack(2)
    gather1(2)
    gather2(1)
    heads(1)
    unpack(3)
    gather1(3)
    heads(5)
    scan1()
    gather3(0)
    gather4(0)
    arrive("eg", "eu", "ed")
    experts(0)
    sum1(0)
    gather2(2)
    gather3(1)
    sum2(0)
    gather3(4)
    gather2(3)
    gather4(1)
    experts(1)
    sum1(1)
    scan2()
    gather3(2)
    sum2(1)
    sum3(0)
    gather4(2)
    experts(2)
    sum1(2)
    gather3(3)
    sum2(2)
    sum3(1)
    gather4(3)
    experts(3)
    sum1(3)
    gather4(4)
    arrive("sg", "su", "sd")
    shared_expert()
    sum1(4)
    give_back(0)
    scan3()
    sum2(3)
    sum3(2)
    give_back(1)
    finish_heads()
    project_out()
    sum1("a")
    sum2(4)
    sum3(3)
    give_back(2)
    sum2("a")
    sum3(4)
    give_back(3)
    sum3("a")
    total = sum4(4)
    out_a[...] = sum4("a").astype(BF)
    routed = None
    for k in range(CHUNKS):
        take(tiles_of(rrx, k), ("r", k))
        tiles = rrx[8 * k : 8 * k + 8].reshape(128, 512)
        at = slice(128 * k, 128 * k + 128)
        part = dot(sel_hi[at].T, tiles) + dot(sel_lo[at].T, tiles)
        routed = part if routed is None else routed + part
    out_b[...] = (quarter_lanes(routed, 32) + total).astype(BF)
    for k in range(5):
        sent(X.at[k, 0:7], ("g", k))
        sent(Y.at[k, 0:7], ("s", k))
    sent(YA.at[0:7], ("s", "a"))
    sent(atx.at[0:3], "x")
    sent(zrx.at[0:7], "z")
    sent(btx.at[0:3], "b")
    sent(tx.at[0:31], "d")
    sent(rtx.at[0:31], "r")
    assert (len(send_names), len(recv_names)) == (LEAVING, LANDING)


LEAVING, LANDING = 16, 55


def per_device(
    xa, gain_a, wq, wk, wv, decay_down, decay_up, decay_bias, decay_shift, decay_spike,
    rate_down, rate_up, rate_base, head_gain, w_out, xb, gain_b, ids, weights,
    e_gate, e_up, e_down, s_gate, s_up, s_down,
):
    here = pl.BlockSpec(memory_space=pltpu.VMEM)
    away = pl.BlockSpec(memory_space=pl.ANY)
    operands = [
        (xa, away), (gain_a, away), (wq, away), (wk, away), (wv, away),
        (decay_down.T, away), (decay_up, away), (decay_bias[None], away),
        (decay_shift, away), (decay_spike, away), (rate_down.T, away), (rate_up, away),
        (rate_base[None], away), (head_gain, away), (w_out, away), (xb, away),
        (gain_b, away), (ids.T, away), (weights.T, away), (e_gate, away), (e_up, away),
        (e_down, away), (s_gate, away), (s_up, away), (s_down, away),
    ]
    vm = pltpu.VMEM
    sums = lambda n: [
        vm((4, n, 2048), BF), vm((4, n, 2048), BF)] + [vm((n, HALF), BF)] * 8
    stacked = [vm((5,) + s.shape, BF) for s in sums(32)]
    scratch = [
        vm((128, 2048), BF), vm((2048, 768), BF), vm((64, 2048), BF), vm((64, 2048), BF),
        vm((128, 256), F32), vm((128, 256), F32), vm((256, 2048), BF), vm((2, 2048, 256), BF),
        vm((2, 128, 2048), BF), vm((2048, 256), BF), vm((128, 2048), BF),
        vm((2048,), BF), vm((64, 256), BF), vm((1, 256), F32), vm((64, 256), BF), vm((1, 256), F32),
        vm((256,), BF), vm((32, 2048), BF), vm((2048,), BF), vm((2, 256), jnp.int32), vm((2, 32), F32),
        vm((32, 16, 512), BF), vm((32, 16, 512), BF), vm((32, 16, 512), BF), vm((32, 16, 512), BF),
        vm((5, 8, 32, 2048), BF), vm((5, 8, 32, 2048), BF),
        *stacked,
        vm((8, 16, 2048), BF), *sums(16),
        vm((4, 64, 128), F32), vm((4, 128, 128), F32), vm((128, 256), BF),
        vm((4, 64, 128), BF), vm((4, 64, 128), BF), vm((64, 128), BF), vm((8, 64, 128), BF),
        vm((4, 64, 128), BF), vm((4, 64, 128), BF), vm((512, 128), BF), vm((512, 128), BF),
        pltpu.SemaphoreType.DMA((25,)), pltpu.SemaphoreType.DMA((LEAVING,)),
        pltpu.SemaphoreType.DMA((LANDING,)),
    ]
    return pl.pallas_call(
        kernel,
        out_shape=(vm((16, 2048), BF), vm((32, 2048), BF)),
        in_specs=[spec for _, spec in operands],
        out_specs=(here, here),
        scratch_shapes=scratch,
        compiler_params=pltpu.CompilerParams(
            collective_id=0, has_side_effects=True, vmem_limit_bytes=60 * 1024 * 1024
        ),
    )(*[array for array, _ in operands])


def solution(mesh):
    split_mesh = Mesh(mesh.devices.reshape(8, 4, 4, 2), ("z", "x", "y", "c"))
    ep, tp = ("z", "x"), ("y", "c")
    both = ep + tp
    return jax.shard_map(
        per_device,
        mesh=split_mesh,
        in_specs=(
            P(ep, None), P(), P(None, tp), P(None, tp), P(None, tp), P(), P(None, tp), P(tp),
            P(ep, tp), P(ep, tp), P(), P(None, tp), P(tp), P(tp), P(tp, None), P(both, None),
            P(), P(ep, None), P(both, None), P(ep, None, tp), P(ep, None, tp), P(ep, tp, None),
            P(None, tp), P(None, tp), P(tp, None),
        ),
        out_specs=(P(both, None), P(both, None)),
        check_vma=False,
    )
```

time: 87.9 us -> 69.4 us (0.79)
  Pallas kernels: 82.4 us -> 67.3 us
  local copies, waits for them, and re-layouts: 4.7 us -> 1.29 us
    pallas_call x1, Pallas kernels: 82.4 us -> 67.3 us  [per_device(): pl.pallas_call(kernel, out_shape=(vm((16, 2048), BF), vm((32, 2048), BF))...]
    broadcast_in_dim x3 -> x0, local copies, waits for them, and re-layouts: 1.79 us -> none  [the longest x1 0.6 us: per_device(): gain_a[None]]
    unnamed x10 -> x2, local copies, waits for them, and re-layouts: 2.91 us -> 1.29 us
where the time goes in v2:
time: 69.4 us; the launch traced here: 69.3 us
  Pallas kernels  67.3 us (97%)
  local copies, waits for them, and re-layouts  1.29 us (2%)
    pallas_call x1, Pallas kernels, per_device(): pl.pallas_call(kernel, out_shape=(vm((16, 2048), BF), vm((32, 2048), BF))...  67.3 us

profile of v2, /device:TPU:1, one launch (start us, length us, event | category | flops | bytes accessed | tf_op | source)
XLA Modules:
  0.0 69.3 jit_solution(9618180655963672478)
XLA Ops:
  0.6 67.3 %shard_map.248 = (bf16[16,2048]{1,0:T(8,128)(2,1)S(1)}, bf16[32,2048]{1,0:T(8,128)(2,1)S(1)}) custom-call(bf16[128,2048]{1,0:T(8,128)(2,1)} %xa.1, bf16[2048]{0:T(1024)(128)(2,1)} %h_gain_a.1, bf16[2048,256]{1,0:T(8,128)(2,1)} %wq.1, bf16[2048,256]{1,0:T(8,128)(2,1)} %wk.1, bf16[2048,256]{1,0:T(8,128)(2,1)} %wv.1, bf16[64,2048]{1,0:T(8,128)(2,1)} %bitcast.6, ...), custom_call_target="tpu_custom_call" | custom-call | tf_op jit(solution)/shard_map/pallas_call | solution.py:579
  68.0 0.6 copy.29
  68.6 0.7 copy.30

commit v3 on v2

--- a/solution.py
+++ b/solution.py
@@ -492,8 +492,8 @@
     experts(2)
     sum1(2)
     gather3(3)
+    sum3(1)
     sum2(2)
-    sum3(1)
     gather4(3)
     experts(3)
     sum1(3)
@@ -503,14 +503,14 @@
     sum1(4)
     give_back(0)
     scan3()
+    sum3(2)
     sum2(3)
-    sum3(2)
     give_back(1)
     finish_heads()
     project_out()
     sum1("a")
+    sum3(3)
     sum2(4)
-    sum3(3)
     give_back(2)
     sum2("a")
     sum3(4)

time: 69.4 us -> 67.3 us (0.970)
  Pallas kernels: 67.3 us -> 65.2 us
    pallas_call x1, Pallas kernels: 67.3 us -> 65.2 us  [per_device(): pl.pallas_call(kernel, out_shape=(vm((16, 2048), BF), vm((32, 2048), BF))...]
where the time goes in v3:
time: 67.3 us; the launch traced here: 67.2 us
  Pallas kernels  65.2 us (97%)
  local copies, waits for them, and re-layouts  1.29 us (2%)
    pallas_call x1, Pallas kernels, per_device(): pl.pallas_call(kernel, out_shape=(vm((16, 2048), BF), vm((32, 2048), BF))...  65.2 us

profile of v3, /device:TPU:1, one launch (start us, length us, event | category | flops | bytes accessed | tf_op | source)
XLA Modules:
  0.0 67.2 jit_solution(7050337391331356946)
XLA Ops:
  0.6 65.2 %shard_map.248 = (bf16[16,2048]{1,0:T(8,128)(2,1)S(1)}, bf16[32,2048]{1,0:T(8,128)(2,1)S(1)}) custom-call(bf16[128,2048]{1,0:T(8,128)(2,1)} %xa.1, bf16[2048]{0:T(1024)(128)(2,1)} %h_gain_a.1, bf16[2048,256]{1,0:T(8,128)(2,1)} %wq.1, bf16[2048,256]{1,0:T(8,128)(2,1)} %wk.1, bf16[2048,256]{1,0:T(8,128)(2,1)} %wv.1, bf16[64,2048]{1,0:T(8,128)(2,1)} %bitcast.6, ...), custom_call_target="tpu_custom_call" | custom-call | tf_op jit(solution)/shard_map/pallas_call | solution.py:579
  65.9 0.6 copy.29
  66.5 0.7 copy.30
